TPU v7x, 256 devices: a whole 4x4x8 slice. The times are simulated.
256 devices in a mesh: sp: 64 (over z, y, core), tp: 4 (over x).
Axes of the slice: x: 4, y: 4, z: 8, core: 2. Of those that a mesh axis runs over, the one named last changes fastest.
Arguments:
- queries: bfloat16 [40960, 1024], P('sp', 'tp'), may hold values from -6 to 6
- key_input: bfloat16 [40960, 1024], P('sp', 'tp'), may hold values from -6 to 6
- value_input: bfloat16 [40960, 1024], P('sp', 'tp'), may hold values from -6 to 6
- gate_input: bfloat16 [40960, 1024], P('sp', 'tp'), may hold values from -6 to 6
- log_decay: float32 [8, 40960], P('tp', 'sp'), may hold values from -1.6703125 to 0, as said below
- residual: bfloat16 [40960, 2048], P('sp'), may hold values from -52 to 52
- out_weight: bfloat16 [1024, 2048], P('tp'), may hold values from -0.375 to 0.375
- norm_gain: float32 [2048], replicated, may hold values from 0.3 to 2.7, as said below
- norm_bias: float32 [2048], replicated, may hold values from -1.8 to 1.8
- gate_weight: bfloat16 [2048, 5632], P('sp', 'tp'), may hold values from -0.125 to 0.125
- up_weight: bfloat16 [2048, 5632], P('sp', 'tp'), may hold values from -0.125 to 0.125
- down_weight: bfloat16 [5632, 2048], P('tp', 'sp'), may hold values from -0.078125 to 0.078125
- final_gain: float32 [2048], replicated, may hold values from 0.1 to 1.9
- final_bias: float32 [2048], replicated, may hold values from -1.8 to 1.8
Outputs:
- updated: bfloat16 [40960, 2048], P('sp', 'tp')
Inputs may be any that keep to these rules, and one draw needn't show every extreme that they name: `log_decay`: log-decays, never positive. `norm_gain`: positive gains.
All inputs are finite; a program needn't handle non-finite values.
Results may differ from a plain program's by a relative error of at most 0.023.
Values may be sent and summed in bfloat16 or wider, within the bound.
A program may use at most 128 MiB of HBM per device.

v0:
```python
import jax
import jax.numpy as jnp
from jax import lax
from jax.sharding import Mesh
from jax.sharding import PartitionSpec as P

HD = 128
BLOCK = 128
SP = ("sp_0", "sp_1", "sp_2")


ALPHA = 2.0**0.25
EPS = 1e-05
ROPE_BASE = 10000.0


def sent_together(arrays, axis, dim, along):
    widths = [a.shape[along] for a in arrays]
    both = jnp.concatenate(arrays, axis=along)
    filled = lax.all_gather(both, axis, axis=dim, tiled=True)
    return tuple(jnp.split(filled, [sum(widths[:k]) for k in range(1, len(widths))], axis=along))


def neutral_like(x, identity):
    return jax.tree.map(
        lambda part, zero: jnp.zeros_like(part) + jnp.asarray(zero, part.dtype), x, identity
    )


def entering_2(x, axes, combine, identity):
    before = start = neutral_like(x, identity)
    so_far = x
    for axis in reversed(axes):
        peers, position = (lax.axis_size(axis), lax.axis_index(axis))
        pieces = jax.tree.map(
            lambda part, kind: lax.all_gather(part.astype(kind), axis),
            so_far,
            (jnp.bfloat16, jnp.bfloat16),
        )
        inside, so_far = (start, start)
        for k in range(peers):
            passed = k < position
            so_far = combine(
                so_far, jax.tree.map(lambda part, own: part[k].astype(own.dtype), pieces, x)
            )
            inside = jax.tree.map(lambda new, old: jnp.where(passed, new, old), so_far, inside)
        before = combine(inside, before)
    return before


def cut_along(x, dim, peers):
    before, after = (x.shape[:dim], x.shape[dim + 1 :])
    return jnp.moveaxis(x.reshape(*before, peers, -1, *after), dim, 0)


def summed_on_arrival(x, axis, dim):
    parts = cut_along(x, dim, lax.axis_size(axis))
    arrived = lax.all_to_all(parts, axis, split_axis=0, concat_axis=0, tiled=True)
    return arrived.astype(jnp.float32).sum(axis=0)


def copy_for_each(x, axis):
    peers = lax.axis_size(axis)
    return lax.all_to_all(jnp.broadcast_to(x[None], (peers, *x.shape)), axis, 0, 0, tiled=True)


def taken_together(x, axis):
    everything = copy_for_each(x, axis)
    return jnp.sum(everything, axis=0)


def together(arrays, axis):
    ends = [0]
    for a in arrays:
        ends.append(ends[-1] + a.size)
    so_far = taken_together(jnp.concatenate([a.ravel() for a in arrays]), axis)
    return tuple((so_far[b:e].reshape(a.shape) for a, b, e in zip(arrays, ends, ends[1:])))


def joined_along(parts, dim):
    parts = jnp.moveaxis(parts, 0, dim)
    dims = parts.shape
    return parts.reshape(*dims[:dim], dims[dim] * dims[dim + 1], *dims[dim + 2 :])


def collect(x, axis, dim):
    parts = copy_for_each(x, axis)
    return joined_along(parts, dim)


def rotate(values, positions):
    half = values.shape[-1] // 2
    freqs = ROPE_BASE ** (-2.0 * jnp.arange(half, dtype=jnp.float32) / values.shape[-1])
    angles = positions[:, None] * freqs[None, :]
    cosine = jnp.cos(angles)[:, None, :]
    sine = jnp.sin(angles)[:, None, :]
    first = values[..., :half]
    latter_operand = values[..., half:]
    return jnp.concatenate(
        [first * cosine - latter_operand * sine, first * sine + latter_operand * cosine], axis=-1
    )


def head_norm(retained):
    center = retained - jnp.mean(retained, axis=-1, keepdims=True)
    spread = jnp.mean(center * center, axis=-1, keepdims=True)
    return center * lax.rsqrt(spread + EPS)


def combine_states(earlier, later):
    return (earlier[0] * later[0], later[1] + later[0][:, None, None] * earlier[1])


def shards(
    queries,
    key_input,
    value_input,
    gate_input,
    log_decay,
    residual,
    out_weight,
    norm_gain,
    norm_bias,
    gate_weight,
    up_weight,
    down_weight,
    final_gain,
    final_bias,
):
    full_gate, full_up = sent_together((gate_weight, up_weight), SP, 0, 1)
    rows = queries.shape[0]
    heads_here = queries.shape[1] // HD
    blocks = rows // BLOCK
    offset = lax.axis_index(SP) * rows
    positions = (offset + jnp.arange(rows, dtype=jnp.int32)).astype(jnp.float32)
    shaped = (rows, heads_here, HD)
    per_block = (blocks, BLOCK, heads_here, HD)
    turned_q = (
        rotate(queries.astype(jnp.float32).reshape(shaped), positions)
        .astype(jnp.bfloat16)
        .reshape(per_block)
    )
    turned_k = (
        rotate(key_input.astype(jnp.float32).reshape(shaped), positions)
        .astype(jnp.bfloat16)
        .reshape(per_block)
    )
    value_blocks = value_input.reshape(per_block)
    cumul = jnp.cumsum(
        jnp.transpose(log_decay.reshape(heads_here, blocks, BLOCK), (1, 0, 2)), axis=2
    )
    cumul_rows = jnp.transpose(cumul, (0, 2, 1))
    lower = jnp.arange(BLOCK)[:, None] >= jnp.arange(BLOCK)[None, :]
    gaps = cumul[:, :, :, None] - cumul[:, :, None, :]
    damping = jnp.where(lower[None, None], jnp.exp(jnp.minimum(gaps, 0.0)), 0.0)
    scores = jnp.einsum("nihd,njhd->nhij", turned_q, turned_k, preferred_element_type=jnp.float32)
    weights = (scores * damping).astype(jnp.bfloat16)
    inner = jnp.einsum("nhij,njhe->nihe", weights, value_blocks, preferred_element_type=jnp.float32)
    ending = cumul[:, :, -1]
    value_broadened = value_blocks.astype(jnp.float32)
    keyed = turned_k.astype(jnp.float32) * jnp.exp(ending[:, None, :] - cumul_rows)[:, :, :, None]
    fresh = jnp.einsum("njhd,njhe->nhde", keyed, value_broadened)

    def advance(state, pieces):
        decay_here, fresh_here = pieces
        return (jnp.exp(decay_here)[:, None, None] * state + fresh_here, state)

    local_state, prefixes = lax.scan(
        advance, jnp.zeros((heads_here, HD, HD), jnp.float32), (ending, fresh)
    )
    before = jnp.cumsum(ending, axis=0) - ending
    device_decay = jnp.exp(jnp.sum(ending, axis=0))
    scanned = entering_2(
        (device_decay, local_state),
        SP,
        combine_states,
        (jnp.ones_like(device_decay), jnp.zeros_like(local_state)),
    )
    entering = prefixes + jnp.exp(before)[:, :, None, None] * scanned[1][None]
    query_wide = turned_q.astype(jnp.float32) * jnp.exp(cumul_rows)[:, :, :, None]
    outer = jnp.einsum("nihd,nhde->nihe", query_wide, entering)
    normed = head_norm((inner + outer).reshape(shaped)).reshape(rows, heads_here * HD)
    mixed_heads = (jax.nn.silu(gate_input.astype(jnp.float32)) * normed).astype(jnp.bfloat16)
    partial_value = jnp.dot(mixed_heads, out_weight, preferred_element_type=jnp.float32)
    width = residual.shape[1]
    col_width = width // lax.axis_size("tp")
    col_start = lax.axis_index("tp") * col_width

    def own_columns(array):
        return lax.dynamic_slice_in_dim(array, col_start, col_width, array.ndim - 1)

    mix_cols = summed_on_arrival(partial_value.astype(jnp.bfloat16), "tp", 1).astype(jnp.bfloat16)
    leading_sum = ALPHA * own_columns(residual).astype(jnp.float32) + mix_cols.astype(jnp.float32)
    totals, squares = together(
        (jnp.sum(leading_sum, axis=1), jnp.sum(leading_sum * leading_sum, axis=1)), "tp"
    )
    average = totals / width
    spread = squares / width - average * average
    scaled = (leading_sum - average[:, None]) * lax.rsqrt(spread + EPS)[:, None]
    settled_cols = (scaled * own_columns(norm_gain) + own_columns(norm_bias)).astype(jnp.bfloat16)
    settled = collect(settled_cols, "tp", 1)
    gate_acts = jnp.dot(settled, full_gate, preferred_element_type=jnp.float32)
    lifted = jnp.dot(settled, full_up, preferred_element_type=jnp.float32)
    latent_width = (jax.nn.silu(gate_acts) * lifted).astype(jnp.bfloat16)
    terms = jnp.dot(
        latent_width,
        lax.all_gather(down_weight, SP, axis=1, tiled=True),
        preferred_element_type=jnp.float32,
    )
    ffn_cols = summed_on_arrival(terms.astype(jnp.bfloat16), "tp", 1).astype(jnp.bfloat16)
    second_sum = ALPHA * settled_cols.astype(jnp.float32) + ffn_cols.astype(jnp.float32)
    totals_two, squares_two = together(
        (jnp.sum(second_sum, axis=1), jnp.sum(second_sum * second_sum, axis=1)), "tp"
    )
    average_two = totals_two / width
    spread_two = squares_two / width - average_two * average_two
    scaled_two = (second_sum - average_two[:, None]) * lax.rsqrt(spread_two + EPS)[:, None]
    return (scaled_two * own_columns(final_gain) + own_columns(final_bias)).astype(jnp.bfloat16)


def solution(mesh):
    split = Mesh(mesh.devices.reshape(8, 4, 2, mesh.shape["tp"]), ("sp_0", "sp_1", "sp_2", "tp"))
    placed = (
        P(SP, "tp"),
        P(SP, "tp"),
        P(SP, "tp"),
        P(SP, "tp"),
        P("tp", SP),
        P(SP, None),
        P("tp", None),
        P(),
        P(),
        P(SP, "tp"),
        P(SP, "tp"),
        P("tp", SP),
        P(),
        P(),
    )
    return jax.shard_map(
        shards, mesh=split, in_specs=placed, out_specs=P(SP, "tp"), check_vma=False
    )
```

profile of v0, /device:TPU:24, one launch (start us, length us, event | category | flops | bytes accessed | tf_op | source)
XLA Modules:
  0.0 265.9 jit_solution(10184661899327183531)
XLA Ops:
  6.5 1.7 pad_maximum_fusion.2
  8.3 0.7 all-gather.9.cloned.1.call-update
  9.1 0.7 reshape.337
  9.8 1.5 reduce_window_sum.22
  11.7 0.8 reduce_window_sum.23
  12.5 1.2 copy.117
  13.6 1.1 copy.118
  16.7 0.7 dynamic-slice
  18.5 2.5 all-reduce
  21.9 7.7 %all-gather.2 = bf16[4,1,2]{2,1,0:T(2,128)(2,1)S(1)} all-gather(bf16[1,1,2]{2,1,0:T(2,128)(2,1)S(1)} %convert_bitcast_fusion), channel_id=1, replica_groups=mesh['sp_0'=8,'sp_1'=4,'sp_2'=2,'tp'=4] {'sp_1'}, dimensions={0}, use_global_device_ids=true | all-gather | bytes 20 | tf_op jit(solution)/shard_map/all_gather | solution.py:36
  29.6 1.1 reshape.338
  30.6 18.8 %all-gather.3 = bf16[8,1,2]{2,1,0:T(2,128)(2,1)} all-gather(bf16[1,1,2]{2,1,0:T(2,128)(2,1)S(1)} %fusion.72), channel_id=1, replica_groups=mesh['sp_0'=8,'sp_1'=4,'sp_2'=2,'tp'=4] {'sp_0'}, dimensions={0}, use_global_device_ids=true | all-gather | bytes 36 | tf_op jit(solution)/shard_map/all_gather | solution.py:36
  50.0 3.9 %while.14 = (s32[]{:T(128)}, f32[2,128,128]{2,1,0:T(8,128)S(1)}, f32[5,2,128,128]{3,2,1,0:T(8,128)}, f32[5,2]{1,0:T(8,128)S(1)}, f32[5,2,128,128]{3,2,1,0:T(8,128)S(1)}) while((s32[]{:T(128)}, f32[2,128,128]{2,1,0:T(8,128)S(1)}, f32[5,2,128,128]{3,2,1,0:T(8,128)}, f32[5,2]{1,0:T(8,128)S(1)}, ...), condition=%wide.region_2.3_spmd.clone.clone, body=%wide.region_1.2_spmd.clone.sunk.clone | while | flops 131075 | bytes 655976 | solution.py:168
  54.9 0.8 subtract_exponential_fusion
  55.8 1.9 all-gather
  57.7 0.7 slice_convert_fusion.5
  58.4 0.8 fusion.61
  59.3 13.9 %all_gather.35 = bf16[4,2,128,128]{3,2,1,0:T(8,128)(2,1)S(1)} all-gather(bf16[1,2,128,128]{3,2,1,0:T(8,128)(2,1)S(1)} %fusion.53), channel_id=1, replica_groups=mesh['sp_0'=8,'sp_1'=4,'sp_2'=2,'tp'=4] {'sp_1'}, dimensions={0}, use_global_device_ids=true | all-gather | bytes 327680 | tf_op jit(solution)/shard_map/all_gather | solution.py:36
  73.2 0.7 fusion.63
  73.9 0.7 fusion.70
  74.7 27.0 %all_gather.37 = bf16[8,2,128,128]{3,2,1,0:T(8,128)(2,1)S(1)} all-gather(bf16[1,2,128,128]{3,2,1,0:T(8,128)(2,1)S(1)} %fusion.54), channel_id=1, replica_groups=mesh['sp_0'=8,'sp_1'=4,'sp_2'=2,'tp'=4] {'sp_0'}, dimensions={0}, use_global_device_ids=true | all-gather | bytes 589824 | tf_op jit(solution)/shard_map/all_gather | solution.py:36
  102.1 2.2 convolution_bitcast_fusion
  104.3 1.9 fusion.84
  106.3 0.9 copy.107
  107.6 0.8 mul.487
  108.5 0.8 sub.81
  109.3 1.0 convolution_convert_fusion.1
  110.3 1.7 copy.151
  112.0 4.5 %all-to-all-start = ((bf16[4,640,512]{2,1,0:T(8,128)(2,1)}), bf16[4,640,512]{2,1,0:T(8,128)(2,1)}, u32[]{:S(2)}, u32[]{:S(2)}) async-start(bf16[4,640,512]{2,1,0:T(8,128)(2,1)} %bitcast.170), calls=%async_computation | async-start | bytes 5242880 | tf_op jit(solution)/shard_map/all_to_all | solution.py:58
  116.6 28.1 %all-to-all-done = bf16[4,640,512]{2,1,0:T(8,128)(2,1)} async-done(((bf16[4,640,512]{2,1,0:T(8,128)(2,1)}), bf16[4,640,512]{2,1,0:T(8,128)(2,1)}, u32[]{:S(2)}, u32[]{:S(2)}) %all-to-all-start) | async-done | bytes 2621472 | tf_op jit(solution)/shard_map/all_to_all | solution.py:58
  144.7 2.5 reduce_sum.108
  147.3 1.5 fusion.14
  149.4 3.3 %all-to-all-start.1 = ((f32[4,1,1280]{2,1,0:T(1,128)}), f32[4,1,1280]{2,1,0:T(1,128)S(1)}, u32[]{:S(2)}, u32[]{:S(2)}) async-start(f32[4,1,1280]{2,1,0:T(1,128)} %broadcast_in_dim.16), calls=%async_computation.1 | async-start | bytes 40960 | tf_op jit(solution)/shard_map/all_to_all | solution.py:64
  152.6 0.8 dynamic_slice.24
  153.4 0.8 dynamic_slice.25
  154.2 3.8 %all-to-all-done.1 = f32[4,1,1280]{2,1,0:T(1,128)S(1)} async-done(((f32[4,1,1280]{2,1,0:T(1,128)}), f32[4,1,1280]{2,1,0:T(1,128)S(1)}, u32[]{:S(2)}, u32[]{:S(2)}) %all-to-all-start.1) | async-done | bytes 20512 | tf_op jit(solution)/shard_map/all_to_all | solution.py:64
  158.0 1.5 add_convert_fusion.1
  160.0 29.4 %all_to_all.27 = bf16[4,640,512]{1,2,0:T(8,128)(2,1)} all-to-all(bf16[4,640,512]{1,2,0:T(8,128)(2,1)S(1)} %broadcast_in_dim.21), channel_id=1, replica_groups=mesh['sp_0'=8,'sp_1'=4,'sp_2'=2,'tp'=4] {'tp'}, dimensions={0} | all-to-all | bytes 5242880 | tf_op jit(solution)/shard_map/all_to_all | solution.py:64
  189.4 9.5 %fusion.4 = f32[640,1408]{1,0:T(8,128)} fusion(bf16[640,2048]{0,1:T(8,128)(2,1)} %bitcast.172, bf16[2048,2816]{1,0:T(8,128)(2,1)} %all-gather.7.cloned.1.call-done), kind=kOutput, calls=%fused_computation.7 | convolution fusion | flops 3690987520 | bytes 11993088 | tf_op jit(solution)/shard_map/dot_general | solution.py:202
  198.9 16.4 %convolution_convert_fusion = bf16[640,2048]{1,0:T(8,128)(2,1)} fusion(bf16[1408,2048]{0,1:T(8,128)(2,1)} %all-gather.9.cloned.1.call-done, bf16[640,2048]{0,1:T(8,128)(2,1)} %bitcast.173, bf16[2048,2816]{1,0:T(8,128)(2,1)} %all-gather.7.cloned.1.call-done, f32[640,1408]{1,0:T(8,128)} %fusion.4), kind=kOutput, calls=%fused_computation.11 | convolution fusion | flops 7388692480 | bytes 20381696 | tf_op jit(solution)/shard_map/dot_general | solution.py:205
  215.2 1.9 copy.150
  217.2 28.5 %all_to_all.28 = bf16[4,640,512]{2,1,0:T(8,128)(2,1)} all-to-all(bf16[4,640,512]{2,1,0:T(8,128)(2,1)S(1)} %bitcast.171), channel_id=1, replica_groups=mesh['sp_0'=8,'sp_1'=4,'sp_2'=2,'tp'=4] {'tp'}, dimensions={0} | all-to-all | bytes 5242880 | tf_op jit(solution)/shard_map/all_to_all | solution.py:58
  245.7 2.5 reduce_sum.112
  249.2 3.3 %all-to-all-start.4 = ((f32[4,1,1280]{2,1,0:T(1,128)}), f32[4,1,1280]{2,1,0:T(1,128)S(1)}, u32[]{:S(2)}, u32[]{:S(2)}) async-start(f32[4,1,1280]{2,1,0:T(1,128)} %broadcast_in_dim.22), calls=%async_computation.4 | async-start | bytes 40960 | tf_op jit(solution)/shard_map/all_to_all | solution.py:64
  252.5 0.8 dynamic_slice.26
  253.2 0.8 dynamic_slice.27
  254.0 3.8 %all-to-all-done.4 = f32[4,1,1280]{2,1,0:T(1,128)S(1)} async-done(((f32[4,1,1280]{2,1,0:T(1,128)}), f32[4,1,1280]{2,1,0:T(1,128)S(1)}, u32[]{:S(2)}, u32[]{:S(2)}) %all-to-all-start.4) | async-done | bytes 20512 | tf_op jit(solution)/shard_map/all_to_all | solution.py:64
  257.9 1.2 add_convert_fusion
  (78 shorter events, 12.4 us)
Async XLA Ops:
  6.5 102.8 %copy-start = (bf16[256,2048]{1,0:T(8,128)(2,1)S(1)}, bf16[256,2048]{1,0:T(8,128)(2,1)}, u32[]{:S(2)}) copy-start(bf16[256,2048]{1,0:T(8,128)(2,1)} %param.22) | copy-start | bytes 3145732
  6.5 182.8 %all-gather.7.cloned.1.call-start = ((), (), s32[]{:S(2)}) async-start(), calls=%async_computation.5 | async-start | bytes 11714560 | tf_op jit(solution)/shard_map/all_gather | solution.py:20
  8.3 190.6 %all-gather.9.cloned.1.call-start = ((), (), s32[]{:S(2)}) async-start(), calls=%async_computation.6 | async-start | bytes 5857280 | tf_op jit(solution)/shard_map/all_gather | solution.py:207
  12.5 4.2 %copy-start.4 = (u32[256]{0:T(256)S(1)}, u32[256]{0:T(256)}, u32[]{:S(2)}) copy-start(u32[256]{0:T(256)} %constant.99) | copy-start | bytes 3076
  21.0 0.6 copy-start.2
  54.9 47.2 %copy-start.1 = (f32[5,2,128,128]{3,2,1,0:T(8,128)S(1)}, f32[5,2,128,128]{3,2,1,0:T(8,128)}, u32[]{:S(2)}) copy-start(f32[5,2,128,128]{3,2,1,0:T(8,128)} %get-tuple-element.33) | copy-start | bytes 1966084
  106.2 3.1 %copy-start.3 = (bf16[640,256]{1,0:T(8,128)(2,1)S(1)}, bf16[640,256]{1,0:T(8,128)(2,1)}, u32[]{:S(2)}) copy-start(bf16[640,256]{1,0:T(8,128)(2,1)} %param.19) | copy-start | bytes 983044
  112.0 32.7 %all-to-all-start = ((bf16[4,640,512]{2,1,0:T(8,128)(2,1)}), bf16[4,640,512]{2,1,0:T(8,128)(2,1)}, u32[]{:S(2)}, u32[]{:S(2)}) async-start(bf16[4,640,512]{2,1,0:T(8,128)(2,1)} %bitcast.170), calls=%async_computation | async-start | bytes 5242880 | tf_op jit(solution)/shard_map/all_to_all | solution.py:58
  149.4 8.6 %all-to-all-start.1 = ((f32[4,1,1280]{2,1,0:T(1,128)}), f32[4,1,1280]{2,1,0:T(1,128)S(1)}, u32[]{:S(2)}, u32[]{:S(2)}) async-start(f32[4,1,1280]{2,1,0:T(1,128)} %broadcast_in_dim.16), calls=%async_computation.1 | async-start | bytes 40960 | tf_op jit(solution)/shard_map/all_to_all | solution.py:64
  249.2 8.6 %all-to-all-start.4 = ((f32[4,1,1280]{2,1,0:T(1,128)}), f32[4,1,1280]{2,1,0:T(1,128)S(1)}, u32[]{:S(2)}, u32[]{:S(2)}) async-start(f32[4,1,1280]{2,1,0:T(1,128)} %broadcast_in_dim.22), calls=%async_computation.4 | async-start | bytes 40960 | tf_op jit(solution)/shard_map/all_to_all | solution.py:64
Sparse Core Ops, SparseCore 0:
  10.1 93.1 all-gather.6
  106.0 77.2 all-gather.8
where the time goes:
time: 267 us; the launch traced here: 266 us
  blocking collectives  130 us (49%)
  waiting for transfers between devices  36.5 us (14%)
  matrix products  31.5 us (12%)
  other arithmetic  23.6 us (9%)
  local copies, waits for them, and re-layouts  19.1 us (7%)
  between operations  14.5 us (5%)
  starting transfers between devices  11.1 us (4%)
    all_gather x5, blocking collectives, entering_2(): lax.all_gather(part.astype(kind), axis)  69.2 us
    all_to_all x1, blocking collectives, copy_for_each(): lax.all_to_all(jnp.broadcast_to(x[None], (peers, *x.shape)), axis, 0, 0,...  29.4 us
    all_to_all x1, blocking collectives, summed_on_arrival(): lax.all_to_all(parts, axis, split_axis=0, concat_axis=0, tiled=True)  28.5 us
    all_to_all x1, waiting for transfers between devices, summed_on_arrival(): lax.all_to_all(parts, axis, split_axis=0, concat_axis=0, tiled=True)  28.1 us
    dot_general x1, matrix products, shards(): jnp.dot(latent_width, lax.all_gather(down_weight, SP, axis=1, tiled=True)...  16.4 us
    dot_general x1, matrix products, shards(): gate_acts = jnp.dot(settled, full_gate, preferred_element_type=jnp.float32)  9.48 us
    all_to_all x2, waiting for transfers between devices, copy_for_each(): lax.all_to_all(jnp.broadcast_to(x[None], (peers, *x.shape)), axis, 0, 0,...  7.65 us
    all_to_all x2, starting transfers between devices, copy_for_each(): lax.all_to_all(jnp.broadcast_to(x[None], (peers, *x.shape)), axis, 0, 0,...  6.51 us
  transfers between devices with their start and end apart: 5, of which 3 were waited for; matrix products, arithmetic and copies ran while one was open for 18% of the time, Pallas kernels for 0%

commit v1 on v0

v1 whole, which is shorter than its diff:
```python
import jax
import jax.numpy as jnp
from jax import lax
from jax.experimental import pallas as pl
from jax.experimental.pallas import tpu as pltpu
from jax.sharding import Mesh
from jax.sharding import PartitionSpec as P

HD = 128
BLOCK = 128
SP = ("sp_0", "sp_1", "sp_2")
ALPHA = 2.0**0.25
EPS = 1e-05
ROPE_BASE = 10000.0
ROWS = 640
NB = ROWS // BLOCK
F32 = jnp.float32
BF16 = jnp.bfloat16
MSG = 144
NSEM = 224


class Net:
    def __init__(self, send, recv):
        self.send, self.recv, self.made = send, recv, []

    def copy(self, src, dst, **where):
        k = len(self.made)
        made = pltpu.make_async_remote_copy(
            src_ref=src,
            dst_ref=dst,
            send_sem=self.send.at[k],
            recv_sem=self.recv.at[k],
            device_id=where,
            device_id_type=pl.DeviceIdType.MESH,
        )
        made.start()
        self.made.append(made)
        return made

    def same(self, ref, **where):
        return self.copy(ref, ref, **where)


def nt(a, b):
    return lax.dot_general(a, b, (((1,), (1,)), ((), ())), preferred_element_type=F32)


def tn(a, b):
    return lax.dot_general(a, b, (((0,), (0,)), ((), ())), preferred_element_type=F32)


def nn(a, b):
    return jnp.dot(a, b, preferred_element_type=F32)


def write_message(ref, state, decay):
    ref[0:HD] = state.astype(BF16)
    high = jnp.broadcast_to(decay, (16, HD)).astype(BF16).astype(F32)
    row = lax.broadcasted_iota(jnp.int32, (16, HD), 0)
    rest = jnp.broadcast_to(decay, (16, HD)) - high
    ref[HD:MSG] = jnp.where(row == 0, high, jnp.where(row == 1, rest, 0.0)).astype(BF16)


def read_message(ref):
    tail = ref[HD:MSG].astype(F32)
    return ref[0:HD].astype(F32), tail[0:1] + tail[1:2]


def kernel(
    q_ref, k_ref, v_ref, g_ref, ld_ref, cos_ref, sin_ref, res_ref, ow_ref,
    gate_ref, up_ref, down_ref, ng_ref, nb_ref, fg_ref, fb_ref,
    out_ref,
    w, ow, mx, qt, kt, inner, prefix, st, stp, ybuf, zbuf, ent,
    total, settled, hidden, via_out, via_in, part_out, part_in, own_part, stat, local_sem,
    send_sem, recv_sem,
):
    z, y, c, x = (lax.axis_index(a) for a in ("sp_0", "sp_1", "sp_2", "tp"))
    zo = [lax.rem(z + k, 8) for k in range(8)]
    yo = [lax.rem(y + k, 4) for k in range(4)]
    xo = [lax.rem(x + k, 4) for k in range(4)]
    zp, zm, yp, ym, xp, xm = zo[1], zo[7], yo[1], yo[3], xo[1], xo[3]
    pc = 1 - c
    barrier = pltpu.get_barrier_semaphore()
    peers = [{"sp_0": zo[k]} for k in range(1, 8)] + [{"sp_1": yo[k]} for k in range(1, 4)]
    peers += [{"tp": xo[k]} for k in range(1, 4)] + [{"sp_2": pc}]
    for peer in peers:
        pl.semaphore_signal(barrier, inc=1, device_id=peer, device_id_type=pl.DeviceIdType.MESH)
    pl.semaphore_wait(barrier, len(peers))

    net = Net(send_sem, recv_sem)
    own = (gate_ref, up_ref, down_ref)
    local = []

    def here(src, dst):
        made = pltpu.make_async_copy(src, dst, local_sem.at[len(local)])
        made.start()
        local.append(made)

    def shard(m, zi, yi):
        return w.at[m, zi, yi, c]

    low, upper = pl.ds(0, 16), pl.ds(16, 16)

    def z_then_y(m):
        mine = shard(m, z, y)
        up, down = net.copy(own[m], mine, sp_0=zp), net.copy(own[m], mine, sp_0=zm)
        side = {0: (net.copy(own[m], mine, sp_1=yp), net.copy(own[m], mine, sp_1=ym))}
        second = []

        def onward(k):
            left, right = side[k]
            left.wait_recv()
            right.wait_recv()
            from_left, from_right = shard(m, zo[k], ym), shard(m, zo[k], yp)
            if k in (0, 4):
                second.append(net.same(from_left.at[low], sp_1=yp))
                second.append(net.same(from_right.at[upper], sp_1=ym))
            elif k < 4:
                second.append(net.same(from_left, sp_1=yp))
            else:
                second.append(net.same(from_right, sp_1=ym))

        yield
        for k in (1, 2, 3):
            up.wait_recv()
            down.wait_recv()
            below, above = shard(m, zo[8 - k], y), shard(m, zo[k], y)
            if k < 3:
                up, down = net.same(below, sp_0=zp), net.same(above, sp_0=zm)
            else:
                up = net.same(below.at[low], sp_0=zp)
                down = net.same(above.at[upper], sp_0=zm)
            side[8 - k] = (net.same(below, sp_1=yp), net.same(below, sp_1=ym))
            side[k] = (net.same(above, sp_1=yp), net.same(above, sp_1=ym))
            yield
            for done in ((0,), (1, 7), (2, 6))[k - 1]:
                onward(done)
            yield
        up.wait_recv()
        down.wait_recv()
        far = shard(m, zo[4], y)
        side[4] = (net.same(far, sp_1=yp), net.same(far, sp_1=ym))
        last = [net.same(w.at[m, :, y, c], sp_2=pc)]
        yield
        onward(3)
        onward(5)
        yield
        onward(4)
        last.append(net.same(w.at[m, :, ym, c], sp_2=pc))
        last.append(net.same(w.at[m, :, yp, c], sp_2=pc))
        yield
        for made in second:
            made.wait_recv()
        last.append(net.same(w.at[m, :, yo[2], c], sp_2=pc))
        yield
        for made in last:
            made.wait_recv()

    def y_then_z(m):
        mine = shard(m, z, y)
        up, down = net.copy(own[m], mine, sp_1=yp), net.copy(own[m], mine, sp_1=ym)
        yield
        up.wait_recv()
        down.wait_recv()
        up = net.same(shard(m, z, ym).at[low], sp_1=yp)
        down = net.same(shard(m, z, yp).at[upper], sp_1=ym)
        yield
        up.wait_recv()
        down.wait_recv()
        row = w.at[m, z, :, c]
        up, down = net.same(row, sp_0=zp), net.same(row, sp_0=zm)
        last = [net.same(row, sp_2=pc)]
        yield
        for k in (1, 2, 3):
            up.wait_recv()
            down.wait_recv()
            below, above = w.at[m, zo[8 - k], :, c], w.at[m, zo[k], :, c]
            if k < 3:
                up, down = net.same(below, sp_0=zp), net.same(above, sp_0=zm)
            else:
                up = net.same(w.at[m, zo[5], pl.ds(0, 2), c], sp_0=zp)
                down = net.same(w.at[m, zo[3], pl.ds(2, 2), c], sp_0=zm)
            last += [net.same(below, sp_2=pc), net.same(above, sp_2=pc)]
            yield
        up.wait_recv()
        down.wait_recv()
        last.append(net.same(w.at[m, zo[4], :, c], sp_2=pc))
        yield
        for made in last:
            made.wait_recv()

    def out_rows():
        mine = ow.at[x, c]
        up, down = net.copy(ow_ref.at[c], mine, tp=xp), net.copy(ow_ref.at[c], mine, tp=xm)
        yield
        up.wait_recv()
        down.wait_recv()
        up = net.same(ow.at[xm, c, pl.ds(0, 64)], tp=xp)
        down = net.same(ow.at[xp, c, pl.ds(64, 64)], tp=xm)
        last = [net.same(ow.at[xm, c], sp_2=pc), net.same(ow.at[xp, c], sp_2=pc)]
        yield
        up.wait_recv()
        down.wait_recv()
        last.append(net.same(ow.at[xo[2], c], sp_2=pc))
        yield
        for made in last:
            made.wait_recv()

    def go(*gens):
        for gen in gens:
            next(gen, None)

    def finish(gen):
        for _ in gen:
            pass

    for m in range(3):
        here(own[m], shard(m, z, y))
    here(ow_ref, ow.at[x])
    gates, ups, downs, outs = z_then_y(0), y_then_z(1), z_then_y(2), out_rows()
    go(gates, ups, outs)

    cols = [pl.ds(h * HD, HD) for h in range(2)]
    rows = [pl.ds(n * BLOCK, BLOCK) for n in range(NB)]
    at_row = lax.broadcasted_iota(jnp.int32, (BLOCK, BLOCK), 0)
    at_col = lax.broadcasted_iota(jnp.int32, (BLOCK, BLOCK), 1)
    lower = at_row >= at_col
    ones_low = jnp.where(lower, 1.0, 0.0)
    ld = ld_ref[...]
    cum_t = lax.dot_general(
        ones_low, ld, (((1,), (1,)), ((), ())),
        precision=lax.Precision.HIGHEST, preferred_element_type=F32,
    )
    cum = lax.dot_general(
        ld, ones_low, (((1,), (1,)), ((), ())),
        precision=lax.Precision.HIGHEST, preferred_element_type=F32,
    )

    def turned(ref, n, h):
        a = ref[rows[n], cols[h]].astype(F32)
        return (a * cos_ref[rows[n]] + pltpu.roll(a, 64, 1) * sin_ref[rows[n]]).astype(BF16)

    before = {}
    for h in range(2):
        state = jnp.zeros((HD, HD), F32)
        so_far = jnp.zeros((1, 1), F32)
        for n in range(NB):
            r = h * NB + n
            key = turned(k_ref, n, h)
            kt[rows[n], cols[h]] = key
            end = cum[r : r + 1, BLOCK - 1 : BLOCK]
            keyed = (key.astype(F32) * jnp.exp(end - cum_t[:, r : r + 1])).astype(BF16)
            prefix[r] = state
            before[r] = so_far
            state = jnp.exp(end) * state + tn(keyed, v_ref[rows[n], cols[h]])
            so_far = so_far + end
        write_message(st.at[h], state, jnp.exp(so_far))
    core_swap = net.copy(st, stp, sp_2=pc)
    for made in local:
        made.wait()
    go(gates)

    def inside(h, n):
        r = h * NB + n
        query = turned(q_ref, n, h)
        qt[rows[n], cols[h]] = query
        gap = cum_t[:, r : r + 1] - cum[r : r + 1, :]
        damping = jnp.where(lower, jnp.exp(jnp.minimum(gap, 0.0)), 0.0)
        weights = (nt(query, kt[rows[n], cols[h]]) * damping).astype(BF16)
        inner[rows[n], cols[h]] = nn(weights, v_ref[rows[n], cols[h]])

    inside(0, 0)
    core_swap.wait_recv()
    mine_s, mine_d = read_message(st.at[c])
    peer_s, peer_d = read_message(stp.at[c])
    first = c == 0
    s0, s1 = jnp.where(first, mine_s, peer_s), jnp.where(first, peer_s, mine_s)
    d1 = jnp.where(first, peer_d, mine_d)
    write_message(ybuf.at[0], d1 * s0 + s1, mine_d * peer_d)
    y_sends = [net.copy(ybuf.at[0], ybuf.at[k], sp_1=yo[k]) for k in (1, 3, 2)]
    go(ups)
    for n in range(1, NB):
        inside(0, n)
    go(gates)

    def running(buf, count, place):
        run, decay = jnp.zeros((HD, HD), F32), jnp.ones((1, HD), F32)
        ahead, ahead_decay = run, decay
        for i in range(count):
            passed = i == place
            ahead = jnp.where(passed, run, ahead)
            ahead_decay = jnp.where(passed, decay, ahead_decay)
            s, d = read_message(buf.at[lax.rem(place + count - i, count)])
            run, decay = d * run + s, d * decay
        return ahead, ahead_decay, run, decay

    for made in y_sends:
        made.wait_recv()
    ahead_y, decay_y, plane, plane_decay = running(ybuf, 4, y)
    write_message(zbuf.at[0], plane, plane_decay)
    z_sends = [net.copy(zbuf.at[0], zbuf.at[k], sp_0=zo[k]) for k in (1, 7, 2, 6, 3, 5, 4)]
    go(gates, ups, outs, downs)
    for n in range(NB):
        inside(1, n)
    go(gates)
    for made in z_sends:
        made.wait_recv()
    ahead_z = running(zbuf, 8, z)[0]
    ent[c] = decay_y * ahead_z + ahead_y
    ent_swap = net.same(ent.at[c], sp_2=pc)
    go(gates, downs, ups)
    ent_swap.wait_recv()
    entering = []
    for h in range(2):
        s, d = read_message(stp.at[h])
        entering.append(jnp.where(c == 1, d * ent[h] + s, ent[h]))

    my_cols = pl.ds(pl.multiple_of(x * 256, 256), 256)
    mixed = []
    for n in range(NB):
        for h in range(2):
            r = h * NB + n
            held = prefix[r] + jnp.exp(before[r]) * entering[h]
            wide = (qt[rows[n], cols[h]].astype(F32) * jnp.exp(cum_t[:, r : r + 1])).astype(BF16)
            kept = inner[rows[n], cols[h]] + nn(wide, held.astype(BF16))
            center = kept - jnp.mean(kept, axis=-1, keepdims=True)
            spread = jnp.mean(center * center, axis=-1, keepdims=True)
            gate = g_ref[rows[n], cols[h]].astype(F32)
            value = gate / (1.0 + jnp.exp(-gate)) * (center * lax.rsqrt(spread + EPS))
            mx[rows[n], pl.ds(pl.multiple_of(x * 256 + h * HD, HD), HD)] = value.astype(BF16)
        block = mx.at[rows[n], my_cols]
        mixed.append((net.same(block, tp=xp), net.same(block, tp=xm)))
    go(gates, downs, ups, outs)
    far_mixed = []
    left_cols = pl.ds(pl.multiple_of(xm * 256, 256), 256)
    right_cols = pl.ds(pl.multiple_of(xp * 256, 256), 256)
    for n in range(NB):
        for made in mixed[n]:
            made.wait_recv()
        far_mixed.append(net.same(mx.at[pl.ds(n * BLOCK, 64), left_cols], tp=xp))
        far_mixed.append(net.same(mx.at[pl.ds(n * BLOCK + 64, 64), right_cols], tp=xm))
    go(gates, downs, ups)
    finish(outs)
    for made in far_mixed:
        made.wait_recv()
    go(gates, downs)

    @pl.loop(0, 8)
    def _(j):
        span = pl.ds(pl.multiple_of(j * 256, 256), 256)
        mix = nn(mx[...], ow[:, :, :, span].reshape(1024, 256))
        total[:, span] = ALPHA * res_ref[:, span].astype(F32) + mix

    go(gates, downs, ups)

    @pl.loop(0, 20)
    def _(i):
        span = pl.ds(pl.multiple_of(i * 32, 32), 32)
        row = total[span]
        center = row - jnp.mean(row, axis=-1, keepdims=True)
        spread = jnp.mean(center * center, axis=-1, keepdims=True)
        settled[span] = (center * lax.rsqrt(spread + EPS) * ng_ref[...] + nb_ref[...]).astype(BF16)

    go(downs)
    finish(gates)
    go(downs)
    finish(ups)

    def hidden_part(span, width):
        acts = settled[...]
        gate = nn(acts, w[0, :, :, :, :, span].reshape(2048, width))
        lift = nn(acts, w[1, :, :, :, :, span].reshape(2048, width))
        hidden[:, span] = (gate / (1.0 + jnp.exp(-gate)) * lift).astype(BF16)

    @pl.loop(0, 5)
    def _(j):
        hidden_part(pl.ds(pl.multiple_of(j * 256, 256), 256), 256)

    hidden_part(pl.ds(1280, 128), 128)
    finish(downs)

    def down_part(lo, size, dest):
        return nt(hidden[lo : lo + size], w[2, pl.ds(2 * dest, 2)].reshape(512, 1408))

    half = ROWS // 2
    via_out[0] = down_part(0, half, xo[2]).astype(BF16)
    via = [net.copy(via_out.at[0], via_in.at[0], tp=xp)]
    via_out[1] = down_part(half, half, xo[2]).astype(BF16)
    via.append(net.copy(via_out.at[1], via_in.at[1], tp=xm))
    sums = []
    part_out[0, 1] = down_part(half, half, xp).astype(BF16)
    sums.append(net.copy(part_out.at[0, 1], part_in.at[0, 1], tp=xp))
    part_out[1, 0] = down_part(0, half, xm).astype(BF16)
    sums.append(net.copy(part_out.at[1, 0], part_in.at[1, 0], tp=xm))
    here_part = down_part(0, half, xp)
    via[0].wait_recv()
    part_out[0, 0] = (here_part + via_in[0].astype(F32)).astype(BF16)
    sums.append(net.copy(part_out.at[0, 0], part_in.at[0, 0], tp=xp))
    here_part = down_part(half, half, xm)
    via[1].wait_recv()
    part_out[1, 1] = (here_part + via_in[1].astype(F32)).astype(BF16)
    sums.append(net.copy(part_out.at[1, 1], part_in.at[1, 1], tp=xm))
    own_cols = pl.ds(pl.multiple_of(x * 512, 512), 512)
    own_part[0:half] = down_part(0, half, x) + ALPHA * settled[0:half, own_cols].astype(F32)
    own_part[half:ROWS] = down_part(half, half, x) + ALPHA * settled[half:ROWS, own_cols].astype(F32)
    for made in sums:
        made.wait_recv()
    lane = lax.broadcasted_iota(jnp.int32, (BLOCK, BLOCK), 1)
    for n in range(NB):
        a = n * BLOCK
        pieces = []
        for lo in (a, a + 64):
            part, off = lo // half, lo % half
            pieces.append(
                own_part[lo : lo + 64]
                + part_in[0, part, off : off + 64].astype(F32)
                + part_in[1, part, off : off + 64].astype(F32)
            )
        second = jnp.concatenate(pieces, axis=0)
        own_part[a : a + BLOCK] = second
        s = jnp.sum(second, axis=-1, keepdims=True)
        q = jnp.sum(second * second, axis=-1, keepdims=True)
        both = jnp.where(lane == 0, s, jnp.where(lane == 1, q, 0.0))
        stat[0, n] = both.T[0:8]
    stats = [net.copy(stat.at[0], stat.at[k], tp=xo[k]) for k in (1, 3, 2)]
    for made in stats:
        made.wait_recv()
    for n in range(NB):
        a = n * BLOCK
        sums_t = stat[0, n] + stat[1, n] + stat[2, n] + stat[3, n]
        wide = jnp.concatenate([sums_t] + [jnp.zeros((120, BLOCK), F32)], axis=0).T
        mean = wide[:, 0:1] / 2048.0
        spread = wide[:, 1:2] / 2048.0 - mean * mean
        scaled = (own_part[a : a + BLOCK] - mean) * lax.rsqrt(spread + EPS)
        out_ref[a : a + BLOCK] = (scaled * fg_ref[...] + fb_ref[...]).astype(BF16)
    for made in net.made:
        made.wait_send()


def shards(
    queries, key_input, value_input, gate_input, log_decay, residual, out_weight,
    norm_gain, norm_bias, gate_weight, up_weight, down_weight, final_gain, final_bias,
):
    offset = lax.axis_index(SP) * ROWS
    positions = (offset + jnp.arange(ROWS, dtype=jnp.int32)).astype(F32)
    freqs = ROPE_BASE ** (-2.0 * jnp.arange(64, dtype=F32) / HD)
    angles = positions[:, None] * freqs[None, :]
    cosine, sine = jnp.cos(angles), jnp.sin(angles)
    cosines = jnp.concatenate([cosine, cosine], axis=1)
    sines = jnp.concatenate([-sine, sine], axis=1)
    decays = jnp.pad(log_decay.reshape(2 * NB, BLOCK), ((0, 16 - 2 * NB), (0, 0)))
    start = lax.axis_index("tp") * 512
    gain_cols = lax.dynamic_slice_in_dim(final_gain, start, 512)[None]
    bias_cols = lax.dynamic_slice_in_dim(final_bias, start, 512)[None]
    args = (
        queries, key_input, value_input, gate_input, decays, cosines, sines, residual,
        out_weight.reshape(2, 128, 2048), gate_weight, up_weight, down_weight.T,
        norm_gain[None], norm_bias[None], gain_cols, bias_cols,
    )
    vm = pltpu.VMEM
    return pl.pallas_call(
        kernel,
        out_shape=jax.ShapeDtypeStruct((ROWS, 512), BF16),
        in_specs=[pl.BlockSpec(memory_space=pltpu.VMEM)] * len(args),
        out_specs=pl.BlockSpec(memory_space=pltpu.VMEM),
        scratch_shapes=[
            vm((3, 8, 4, 2, 32, 1408), BF16),
            vm((4, 2, 128, 2048), BF16),
            vm((ROWS, 1024), BF16),
            vm((ROWS, 256), BF16),
            vm((ROWS, 256), BF16),
            vm((ROWS, 256), F32),
            vm((2 * NB, HD, HD), F32),
            vm((2, MSG, HD), BF16),
            vm((2, MSG, HD), BF16),
            vm((4, MSG, HD), BF16),
            vm((8, MSG, HD), BF16),
            vm((2, HD, HD), F32),
            vm((ROWS, 2048), F32),
            vm((ROWS, 2048), BF16),
            vm((ROWS, 1408), BF16),
            vm((2, ROWS // 2, 512), BF16),
            vm((2, ROWS // 2, 512), BF16),
            vm((2, 2, ROWS // 2, 512), BF16),
            vm((2, 2, ROWS // 2, 512), BF16),
            vm((ROWS, 512), F32),
            vm((4, NB, 8, 128), F32),
            pltpu.SemaphoreType.DMA((4,)),
            pltpu.SemaphoreType.DMA((NSEM,)),
            pltpu.SemaphoreType.DMA((NSEM,)),
        ],
        compiler_params=pltpu.CompilerParams(
            collective_id=0, has_side_effects=True, vmem_limit_bytes=66_000_000
        ),
    )(*args)


def solution(mesh):
    split = Mesh(mesh.devices.reshape(8, 4, 2, mesh.shape["tp"]), ("sp_0", "sp_1", "sp_2", "tp"))
    placed = (
        P(SP, "tp"), P(SP, "tp"), P(SP, "tp"), P(SP, "tp"), P("tp", SP), P(SP, None),
        P("tp", None), P(), P(), P(SP, "tp"), P(SP, "tp"), P("tp", SP), P(), P(),
    )
    return jax.shard_map(
        shards, mesh=split, in_specs=placed, out_specs=P(SP, "tp"), check_vma=False
    )
```

time: 267 us -> 132 us (0.49)
  the two profiles are of different devices: /device:TPU:24 before, /device:TPU:1 now
where the time goes in v1:
time: 132 us; the launch traced here: 131 us
  Pallas kernels  123 us (93%)
  local copies, waits for them, and re-layouts  5.28 us (4%)
  other arithmetic  2.33 us (2%)
    pallas_call x1, Pallas kernels, shards(): pl.pallas_call(kernel, out_shape=jax.ShapeDtypeStruct((ROWS, 512), BF16),...  123 us

profile of v1, /device:TPU:1, one launch (start us, length us, event | category | flops | bytes accessed | tf_op | source)
XLA Modules:
  0.0 131.1 jit_solution(5635302018921318497)
XLA Ops:
  0.0 0.0 copy-start
  0.0 1.2 fusion
  1.2 1.1 pad_maximum_fusion
  2.3 1.3 %dynamic_slice.6 = f32[512]{0:T(512)} dynamic-slice(f32[2048]{0:T(1024)} %param.26, s32[]{:T(128)S(6)} %select_n.4), dynamic_slice_sizes={512} | dynamic-slice | bytes 4100 | tf_op jit(solution)/shard_map/dynamic_slice | solution.py:454
  3.7 1.3 %dynamic_slice.7 = f32[512]{0:T(512)} dynamic-slice(f32[2048]{0:T(1024)} %param.27, s32[]{:T(128)S(6)} %select_n.4), dynamic_slice_sizes={512} | dynamic-slice | bytes 4100 | tf_op jit(solution)/shard_map/dynamic_slice | solution.py:455
  5.0 0.0 copy-done
  5.1 0.6 pad.4.ld_ref
  5.7 123.4 %shard_map.136 = bf16[640,512]{1,0:T(8,128)(2,1)} custom-call(bf16[640,256]{1,0:T(8,128)(2,1)} %q_ref.1, bf16[640,256]{1,0:T(8,128)(2,1)} %k_ref.1, bf16[640,256]{1,0:T(8,128)(2,1)} %v_ref.1, bf16[640,256]{1,0:T(8,128)(2,1)} %g_ref.1, f32[16,128]{1,0:T(8,128)} %pad.4.ld_ref, f32[640,128]{1,0:T(8,128)} %get-tuple-element.8.cos_ref, ...), custom_call_target="tpu_custom_call" | custom-call | tf_op jit(solution)/shard_map/pallas_call | solution.py:462
  129.1 2.0 %copy.16 = bf16[640,512]{1,0:T(8,128)(2,1)} copy(bf16[640,512]{1,0:T(8,128)(2,1)} %shard_map.136) | data formatting | bytes 1310720
  (3 shorter events, 0.0 us)
Async XLA Ops:
  0.0 5.0 %copy-start = (f32[2,640]{1,0:T(2,128)S(1)}, f32[2,640]{1,0:T(2,128)}, u32[]{:S(2)}) copy-start(f32[2,640]{1,0:T(2,128)} %param.18) | copy-start | bytes 15364

commit v2 on v1

v2 whole, which is shorter than its diff:
```python
import heapq
import math

import jax
import jax.numpy as jnp
from jax import lax
from jax.experimental import pallas as pl
from jax.experimental.pallas import tpu as pltpu
from jax.sharding import Mesh
from jax.sharding import PartitionSpec as P

HD = 128
BLOCK = 128
SP = ("sp_0", "sp_1", "sp_2")
ALPHA = 2.0**0.25
EPS = 1e-05
ROPE_BASE = 10000.0
ROWS = 640
NB = ROWS // BLOCK
F32 = jnp.float32
BF16 = jnp.bfloat16
MSG = 144
NSEM = 240
SIZE = {"sp_0": 8, "sp_1": 4, "sp_2": 2, "tp": 4}
MARGIN = 0.3
CHUNKS = ((0, 384), (384, 256))


class Flight:
    def __init__(self, made, arrive):
        self.made, self.arrive, self.open = made, arrive, True

    def landed(self):
        if self.open:
            self.made.wait_recv()
            self.open = False


class Net:
    def __init__(self, send, recv, at):
        self.send, self.recv, self.at = send, recv, at
        self.t, self.free, self.tasks, self.made, self.count = 0.0, {}, [], [], 0

    def copy(self, src, dst, axis, k):
        i, size = len(self.made), SIZE[axis]
        k %= size
        made = pltpu.make_async_remote_copy(
            src_ref=src,
            dst_ref=dst,
            send_sem=self.send.at[i],
            recv_sem=self.recv.at[i],
            device_id={axis: self.at[axis][k]},
            device_id_type=pl.DeviceIdType.MESH,
        )
        made.start()
        nbytes = math.prod(src.shape) * src.dtype.itemsize
        hops = min(k, size - k)
        if axis == "sp_2":
            keys, busy, late = [(axis, 1)], nbytes / 6e5, 1.0
        else:
            keys = [(axis, d) for d, far in ((1, k), (-1, size - k)) if far == hops]
            busy, late = hops * nbytes / 4.66e4 / len(keys), 1.0 + 0.75 * hops
        start = max([self.t] + [self.free.get(key, 0.0) for key in keys])
        for key in keys:
            self.free[key] = start + busy
        flight = Flight(made, start + busy + late)
        self.made.append(flight)
        return flight

    def same(self, ref, axis, k):
        return self.copy(ref, ref, axis, k)

    def when(self, flights, action):
        ready = max(f.arrive for f in flights) + MARGIN
        self.count += 1
        heapq.heappush(self.tasks, (ready, self.count, flights, action))

    def pump(self, until=None):
        limit = self.t if until is None else until
        while self.tasks and self.tasks[0][0] <= limit:
            ready, _, flights, action = heapq.heappop(self.tasks)
            self.t = max(self.t, ready)
            for flight in flights:
                flight.landed()
            action()

    def work(self, us):
        self.t += us
        self.pump()

    def need(self, flights):
        while any(f is None for f in flights):
            self.pump(self.tasks[0][0])
        target = max(f.arrive for f in flights)
        self.pump(target)
        self.t = max(self.t, target)
        for flight in flights:
            flight.landed()


def nt(a, b):
    return lax.dot_general(a, b, (((1,), (1,)), ((), ())), preferred_element_type=F32)


def tn(a, b):
    return lax.dot_general(a, b, (((0,), (0,)), ((), ())), preferred_element_type=F32)


def nn(a, b):
    return jnp.dot(a, b, preferred_element_type=F32)


def write_message(ref, state, decay):
    ref[0:HD] = state.astype(BF16)
    high = jnp.broadcast_to(decay, (16, HD)).astype(BF16).astype(F32)
    row = lax.broadcasted_iota(jnp.int32, (16, HD), 0)
    rest = jnp.broadcast_to(decay, (16, HD)) - high
    ref[HD:MSG] = jnp.where(row == 0, high, jnp.where(row == 1, rest, 0.0)).astype(BF16)


def read_message(ref):
    tail = ref[HD:MSG].astype(F32)
    return ref[0:HD].astype(F32), tail[0:1] + tail[1:2]


def kernel(
    q_any, k_ref, v_ref, g_any, ld_ref, cos_ref, sin_ref, res_any, ow_ref,
    gate_ref, up_ref, down_ref, ng_ref, nb_ref, fg_ref, fb_ref,
    out_ref,
    q_ref, g_ref, res_ref, ldp, w, ow, mx, qt, kt, inner, prefix, st, stp, ybuf, zbuf, ent,
    total, settled, hidden, via_out, via_in, part_out, part_in, held_part, own_part, stat,
    local_sem, send_sem, recv_sem,
):
    z, y, c, x = (lax.axis_index(a) for a in ("sp_0", "sp_1", "sp_2", "tp"))
    zo = [lax.rem(z + k, 8) for k in range(8)]
    yo = [lax.rem(y + k, 4) for k in range(4)]
    xo = [lax.rem(x + k, 4) for k in range(4)]
    at = {"sp_0": zo, "sp_1": yo, "sp_2": [c, 1 - c], "tp": xo}
    barrier = pltpu.get_barrier_semaphore()
    peers = [(axis, k) for axis in SIZE for k in range(1, SIZE[axis])]
    for axis, k in peers:
        pl.semaphore_signal(
            barrier, inc=1, device_id={axis: at[axis][k]}, device_id_type=pl.DeviceIdType.MESH
        )
    own = (gate_ref, up_ref, down_ref)
    local = []
    for src, dst in (
        [(own[m], w.at[m, z, y, c]) for m in range(3)]
        + [(ow_ref, ow.at[x]), (q_any, q_ref), (g_any, g_ref), (res_any, res_ref)]
    ):
        made = pltpu.make_async_copy(src, dst, local_sem.at[len(local)])
        made.start()
        local.append(made)

    net = Net(send_sem, recv_sem, at)

    def gather(m, ax_a, ax_b, last):
        la, lb = SIZE[ax_a], SIZE[ax_b]
        low, upper = pl.ds(0, 16), pl.ds(16, 16)
        counts, far_a, far_b = [0] * lb, [], {}

        def shard(a, b):
            if ax_a == "sp_0":
                return w.at[m, zo[a], yo[b], c]
            return w.at[m, zo[b], yo[a], c]

        def landed(a, b):
            counts[b] += 1
            if counts[b] == la:
                block = w.at[m, :, yo[b], c] if ax_a == "sp_0" else w.at[m, zo[b], :, c]
                last.append(net.same(block, "sp_2", 1))

        def along_b(a, k, d):
            b = -k * d % lb
            if k < lb // 2 - 1:
                net.when([net.same(shard(a, b), ax_b, d)], lambda: along_b(a, k + 1, d))
            elif k == lb // 2 - 1:
                if a in (0, la // 2):
                    part = shard(a, b).at[low if d > 0 else upper]
                    far_b.setdefault(a, []).append(net.same(part, ax_b, d))
                    if len(far_b[a]) == 2:
                        net.when(far_b[a], lambda: landed(a, lb // 2))
                elif (a < la // 2) == (d > 0):
                    net.when([net.same(shard(a, b), ax_b, d)], lambda: landed(a, lb // 2))
            landed(a, b)

        def spread(a, src):
            for d in (1, -1):
                flight = net.copy(src, shard(a, 0), ax_b, d)
                net.when([flight], lambda d=d: along_b(a, 1, d))
            landed(a, 0)

        def along_a(k, d):
            a = -k * d % la
            if k < la // 2 - 1:
                net.when([net.same(shard(a, 0), ax_a, d)], lambda: along_a(k + 1, d))
            else:
                far_a.append(net.same(shard(a, 0).at[low if d > 0 else upper], ax_a, d))
                if len(far_a) == 2:
                    net.when(far_a, lambda: spread(la // 2, shard(la // 2, 0)))
            spread(a, shard(a, 0))

        for d in (1, -1):
            flight = net.copy(own[m], shard(0, 0), ax_a, d)
            net.when([flight], lambda d=d: along_a(1, d))
        spread(0, own[m])

    def gather_out(last):
        far = []

        def step(d):
            part = ow.at[xo[-d % 4], c, pl.ds(0 if d > 0 else 64, 64)]
            far.append(net.same(part, "tp", d))
            last.append(net.same(ow.at[xo[-d % 4], c], "sp_2", 1))
            if len(far) == 2:
                net.when(far, lambda: last.append(net.same(ow.at[xo[2], c], "sp_2", 1)))

        for d in (1, -1):
            flight = net.copy(ow_ref.at[c], ow.at[x, c], "tp", d)
            net.when([flight], lambda d=d: step(d))

    def all_of(flights, count):
        while len(flights) < count:
            net.pump(net.tasks[0][0])
        net.need(flights)

    cols = [pl.ds(h * HD, HD) for h in range(2)]
    rows = [pl.ds(n * BLOCK, BLOCK) for n in range(NB)]
    at_row = lax.broadcasted_iota(jnp.int32, (BLOCK, BLOCK), 0)
    at_col = lax.broadcasted_iota(jnp.int32, (BLOCK, BLOCK), 1)
    lower = at_row >= at_col
    ones_low = jnp.where(lower, 1.0, 0.0)
    ldp[...] = jnp.zeros_like(ldp)
    for n in range(NB):
        ldp[2 * n : 2 * n + 2] = ld_ref[:, n * BLOCK : (n + 1) * BLOCK]
    ld = ldp[...]
    cum_t = lax.dot_general(
        ones_low, ld, (((1,), (1,)), ((), ())),
        precision=lax.Precision.HIGHEST, preferred_element_type=F32,
    )
    cum = lax.dot_general(
        ld, ones_low, (((1,), (1,)), ((), ())),
        precision=lax.Precision.HIGHEST, preferred_element_type=F32,
    )

    def turned(ref, n, h):
        a = ref[rows[n], cols[h]].astype(F32)
        return (a * cos_ref[rows[n]] + pltpu.roll(a, 64, 1) * sin_ref[rows[n]]).astype(BF16)

    before = {}
    for h in range(2):
        state = jnp.zeros((HD, HD), F32)
        so_far = jnp.zeros((1, 1), F32)
        for n in range(NB):
            r = n * 2 + h
            key = turned(k_ref, n, h)
            kt[rows[n], cols[h]] = key
            end = cum[r : r + 1, BLOCK - 1 : BLOCK]
            keyed = (key.astype(F32) * jnp.exp(end - cum_t[:, r : r + 1])).astype(BF16)
            prefix[r] = state
            before[r] = so_far
            state = jnp.exp(end) * state + tn(keyed, v_ref[rows[n], cols[h]])
            so_far = so_far + end
        write_message(st.at[h], state, jnp.exp(so_far))

    pl.semaphore_wait(barrier, len(peers))
    core_swap = net.copy(st, stp, "sp_2", 1)
    gates_in, ups_in, downs_in, outs_in = [], [], [], []
    gather(0, "sp_0", "sp_1", gates_in)
    gather(1, "sp_1", "sp_0", ups_in)
    gather_out(outs_in)
    for made in local:
        made.wait()

    def inside(h, n):
        r = n * 2 + h
        query = turned(q_ref, n, h)
        qt[rows[n], cols[h]] = query
        gap = cum_t[:, r : r + 1] - cum[r : r + 1, :]
        damping = jnp.where(lower, jnp.exp(jnp.minimum(gap, 0.0)), 0.0)
        weights = (nt(query, kt[rows[n], cols[h]]) * damping).astype(BF16)
        inner[rows[n], cols[h]] = nn(weights, v_ref[rows[n], cols[h]])
        net.work(0.4)

    inside(0, 0)
    inside(0, 1)
    net.need([core_swap])
    mine_s, mine_d = read_message(st.at[c])
    peer_s, peer_d = read_message(stp.at[c])
    first = c == 0
    s0, s1 = jnp.where(first, mine_s, peer_s), jnp.where(first, peer_s, mine_s)
    d1 = jnp.where(first, peer_d, mine_d)
    write_message(ybuf.at[0], d1 * s0 + s1, mine_d * peer_d)
    y_sends = [net.copy(ybuf.at[0], ybuf.at[k], "sp_1", k) for k in (1, 3, 2)]
    for n in range(2, NB):
        inside(0, n)
    inside(1, 0)
    inside(1, 1)

    def running(buf, count, place):
        run, decay = jnp.zeros((HD, HD), F32), jnp.ones((1, HD), F32)
        ahead, ahead_decay = run, decay
        for i in range(count):
            passed = i == place
            ahead = jnp.where(passed, run, ahead)
            ahead_decay = jnp.where(passed, decay, ahead_decay)
            s, d = read_message(buf.at[lax.rem(place + count - i, count)])
            run, decay = d * run + s, d * decay
        return ahead, ahead_decay, run, decay

    net.need(y_sends)
    ahead_y, decay_y, plane, plane_decay = running(ybuf, 4, y)
    write_message(zbuf.at[0], plane, plane_decay)
    z_sends = [net.copy(zbuf.at[0], zbuf.at[k], "sp_0", k) for k in (1, 7, 2, 6, 3, 5, 4)]
    for n in range(2, NB):
        inside(1, n)
    net.need(z_sends)
    ahead_z = running(zbuf, 8, z)[0]
    ent[c] = decay_y * ahead_z + ahead_y
    ent_swap = net.same(ent.at[c], "sp_2", 1)
    gather(2, "sp_0", "sp_1", downs_in)
    net.need([ent_swap])
    entering = []
    for h in range(2):
        s, d = read_message(stp.at[h])
        entering.append(jnp.where(c == 1, d * ent[h] + s, ent[h]))

    mixed_in = [[] for _ in range(NB)]

    def mixed_step(n, d):
        start = n * BLOCK + (0 if d > 0 else 64)
        where = pl.ds(pl.multiple_of(xo[-d % 4] * 256, 256), 256)
        mixed_in[n].append(net.same(mx.at[pl.ds(start, 64), where], "tp", d))

    for n in range(NB):
        for h in range(2):
            r = n * 2 + h
            held = prefix[r] + jnp.exp(before[r]) * entering[h]
            wide = (qt[rows[n], cols[h]].astype(F32) * jnp.exp(cum_t[:, r : r + 1])).astype(BF16)
            kept = inner[rows[n], cols[h]] + nn(wide, held.astype(BF16))
            center = kept - jnp.mean(kept, axis=-1, keepdims=True)
            spread = jnp.mean(center * center, axis=-1, keepdims=True)
            gate = g_ref[rows[n], cols[h]].astype(F32)
            value = gate / (1.0 + jnp.exp(-gate)) * (center * lax.rsqrt(spread + EPS))
            mx[rows[n], pl.ds(pl.multiple_of(x * 256 + h * HD, HD), HD)] = value.astype(BF16)
        block = mx.at[rows[n], pl.ds(pl.multiple_of(x * 256, 256), 256)]
        for d in (1, -1):
            net.when([net.same(block, "tp", d)], lambda n=n, d=d: mixed_step(n, d))
        net.work(0.6)

    def project(lo, size):
        for part in range(2):

            @pl.loop(4 * part, 4 * part + 4)
            def _(j):
                span = pl.ds(pl.multiple_of(j * 256, 256), 256)
                mix = nn(mx[lo : lo + size], ow[:, :, :, span].reshape(1024, 256))
                total[lo : lo + size, span] = ALPHA * res_ref[lo : lo + size, span].astype(F32) + mix

            net.work(0.0045 * size)

        @pl.loop(lo // 32, (lo + size) // 32)
        def _(i):
            span = pl.ds(pl.multiple_of(i * 32, 32), 32)
            row = total[span]
            center = row - jnp.mean(row, axis=-1, keepdims=True)
            spread = jnp.mean(center * center, axis=-1, keepdims=True)
            scaled = center * lax.rsqrt(spread + EPS)
            settled[span] = (scaled * ng_ref[...] + nb_ref[...]).astype(BF16)

        net.work(0.004 * size)

    def expand(lo, size):
        for j in range(6):
            width = 256 if j < 5 else 128
            span = pl.ds(j * 256, width)
            acts = settled[lo : lo + size]
            gate = nn(acts, w[0, :, :, :, :, span].reshape(2048, width))
            lift = nn(acts, w[1, :, :, :, :, span].reshape(2048, width))
            hidden[lo : lo + size, span] = (gate / (1.0 + jnp.exp(-gate)) * lift).astype(BF16)
            net.work(0.0043 * size)

    own_cols = pl.ds(pl.multiple_of(x * 512, 512), 512)
    last_sums = []

    def contract(lo, size):
        half = size // 2
        top, bottom = (lo, lo + half), (lo + half, lo + size)

        def part(span, dest):
            acts = hidden[span[0] : span[1]]
            value = nt(acts, w[2, pl.ds(2 * dest, 2)].reshape(512, 1408))
            net.t += 0.003 * half
            return value

        def at_(ref, k, span):
            return ref.at[k, span[0] : span[1]]

        sums = []

        def pass_on(k, span, d):
            a, b = span
            joined = held_part[a:b] + via_in[a:b].astype(F32)
            part_out[k, a:b] = joined.astype(BF16)
            sums.append(net.copy(at_(part_out, k, span), at_(part_in, k, span), "tp", d))

        for k, span, d in ((0, top, 1), (1, bottom, -1)):
            a, b = span
            via_out[a:b] = part(span, xo[2]).astype(BF16)
            flight = net.copy(via_out.at[a:b], via_in.at[a:b], "tp", d)
            net.when([flight], lambda k=k, span=span, d=d: pass_on(k, span, d))
        for k, span, d in ((0, bottom, 1), (1, top, -1)):
            a, b = span
            part_out[k, a:b] = part(span, xo[d % 4]).astype(BF16)
            sums.append(net.copy(at_(part_out, k, span), at_(part_in, k, span), "tp", d))
        held_part[top[0] : top[1]] = part(top, xo[1])
        held_part[bottom[0] : bottom[1]] = part(bottom, xo[3])
        net.pump()
        for a, b in (top, bottom):
            own_part[a:b] = part((a, b), x) + ALPHA * settled[a:b, own_cols].astype(F32)
            net.pump()
        return sums

    lane = lax.broadcasted_iota(jnp.int32, (BLOCK, BLOCK), 1)

    def sum_up(lo, size, sums):
        all_of(sums, 4)
        for n in range(lo // BLOCK, (lo + size) // BLOCK):
            a, b = n * BLOCK, (n + 1) * BLOCK
            second = own_part[a:b] + part_in[0, a:b].astype(F32) + part_in[1, a:b].astype(F32)
            own_part[a:b] = second
            s = jnp.sum(second, axis=-1, keepdims=True)
            q = jnp.sum(second * second, axis=-1, keepdims=True)
            both = jnp.where(lane == 0, s, jnp.where(lane == 1, q, 0.0))
            stat[0, n] = both.T[0:8]
        span = pl.ds(lo // BLOCK, size // BLOCK)
        net.work(0.004 * size)
        return [net.copy(stat.at[0, span], stat.at[k, span], "tp", k) for k in (1, 3, 2)]

    def settle(lo, size, stats):
        net.need(stats)
        for n in range(lo // BLOCK, (lo + size) // BLOCK):
            a, b = n * BLOCK, (n + 1) * BLOCK
            sums_t = stat[0, n] + stat[1, n] + stat[2, n] + stat[3, n]
            wide = jnp.concatenate([sums_t] + [jnp.zeros((120, BLOCK), F32)], axis=0).T
            mean = wide[:, 0:1] / 2048.0
            spread = wide[:, 1:2] / 2048.0 - mean * mean
            scaled = (own_part[a:b] - mean) * lax.rsqrt(spread + EPS)
            out_ref[a:b] = (scaled * fg_ref[:, own_cols] + fb_ref[:, own_cols]).astype(BF16)
        net.work(0.004 * size)

    def mixed_ready(lo, size):
        for n in range(lo // BLOCK, (lo + size) // BLOCK):
            all_of(mixed_in[n], 2)

    all_of(outs_in, 3)
    mixed_ready(*CHUNKS[0])
    project(*CHUNKS[0])
    all_of(gates_in, 4)
    all_of(ups_in, 8)
    expand(*CHUNKS[0])
    mixed_ready(*CHUNKS[1])
    project(*CHUNKS[1])
    all_of(downs_in, 4)
    sums_0 = contract(*CHUNKS[0])
    expand(*CHUNKS[1])
    sums_1 = contract(*CHUNKS[1])
    stats_0 = sum_up(*CHUNKS[0], sums_0)
    settle(*CHUNKS[0], stats_0)
    stats_1 = sum_up(*CHUNKS[1], sums_1)
    settle(*CHUNKS[1], stats_1)
    assert not net.tasks
    for flight in net.made:
        flight.made.wait_send()


def shards(
    queries, key_input, value_input, gate_input, log_decay, residual, out_weight,
    norm_gain, norm_bias, gate_weight, up_weight, down_weight, final_gain, final_bias,
):
    offset = lax.axis_index(SP) * ROWS
    positions = (offset + jnp.arange(ROWS, dtype=jnp.int32)).astype(F32)
    freqs = ROPE_BASE ** (-2.0 * jnp.arange(64, dtype=F32) / HD)
    angles = positions[:, None] * freqs[None, :]
    cosine, sine = jnp.cos(angles), jnp.sin(angles)
    cosines = jnp.concatenate([cosine, cosine], axis=1)
    sines = jnp.concatenate([-sine, sine], axis=1)
    args = (
        queries, key_input, value_input, gate_input, log_decay, cosines, sines, residual,
        out_weight.reshape(2, 128, 2048), gate_weight, up_weight, down_weight.T,
        norm_gain[None], norm_bias[None], final_gain[None], final_bias[None],
    )
    vm = pltpu.VMEM
    late = (0, 3, 7)
    placed = [
        pl.BlockSpec(memory_space=pl.ANY if i in late else vm) for i in range(len(args))
    ]
    return pl.pallas_call(
        kernel,
        out_shape=jax.ShapeDtypeStruct((ROWS, 512), BF16),
        in_specs=placed,
        out_specs=pl.BlockSpec(memory_space=pltpu.VMEM),
        scratch_shapes=[
            vm((ROWS, 256), BF16),
            vm((ROWS, 256), BF16),
            vm((ROWS, 2048), BF16),
            vm((16, BLOCK), F32),
            vm((3, 8, 4, 2, 32, 1408), BF16),
            vm((4, 2, 128, 2048), BF16),
            vm((ROWS, 1024), BF16),
            vm((ROWS, 256), BF16),
            vm((ROWS, 256), BF16),
            vm((ROWS, 256), F32),
            vm((2 * NB, HD, HD), F32),
            vm((2, MSG, HD), BF16),
            vm((2, MSG, HD), BF16),
            vm((4, MSG, HD), BF16),
            vm((8, MSG, HD), BF16),
            vm((2, HD, HD), F32),
            vm((ROWS, 2048), F32),
            vm((ROWS, 2048), BF16),
            vm((ROWS, 1408), BF16),
            vm((ROWS, 512), BF16),
            vm((ROWS, 512), BF16),
            vm((2, ROWS, 512), BF16),
            vm((2, ROWS, 512), BF16),
            vm((ROWS, 512), F32),
            vm((ROWS, 512), F32),
            vm((4, NB, 8, 128), F32),
            pltpu.SemaphoreType.DMA((7,)),
            pltpu.SemaphoreType.DMA((NSEM,)),
            pltpu.SemaphoreType.DMA((NSEM,)),
        ],
        compiler_params=pltpu.CompilerParams(
            collective_id=0, has_side_effects=True, vmem_limit_bytes=66_000_000
        ),
    )(*args)


def solution(mesh):
    split = Mesh(mesh.devices.reshape(8, 4, 2, mesh.shape["tp"]), ("sp_0", "sp_1", "sp_2", "tp"))
    placed = (
        P(SP, "tp"), P(SP, "tp"), P(SP, "tp"), P(SP, "tp"), P("tp", SP), P(SP, None),
        P("tp", None), P(), P(), P(SP, "tp"), P(SP, "tp"), P("tp", SP), P(), P(),
    )
    return jax.shard_map(
        shards, mesh=split, in_specs=placed, out_specs=P(SP, "tp"), check_vma=False
    )
```

time: 132 us -> 117 us (0.89)
  Pallas kernels: 123 us -> 113 us
  local copies, waits for them, and re-layouts: 5.28 us -> 1.97 us
    pallas_call x1, Pallas kernels: 123 us -> 113 us  [shards(): pl.pallas_call(kernel, out_shape=jax.ShapeDtypeStruct((ROWS, 512), BF16),...]
    dynamic_slice x2 -> x0, local copies, waits for them, and re-layouts: 2.69 us -> none  [the longest x1 1.35 us: shards(): bias_cols = lax.dynamic_slice_in_dim(final_bias, start, 512)[None]]
where the time goes in v2:
time: 117 us
  Pallas kernels  113 us (97%)
  other arithmetic  2.31 us (2%)
  local copies, waits for them, and re-layouts  1.97 us (2%)
    pallas_call x1, Pallas kernels, shards(): pl.pallas_call(kernel, out_shape=jax.ShapeDtypeStruct((ROWS, 512), BF16),...  113 us

profile of v2, /device:TPU:1, one launch (start us, length us, event | category | flops | bytes accessed | tf_op | source)
XLA Modules:
  0.0 117.1 jit_solution(14048353279893010791)
XLA Ops:
  0.0 1.2 %fusion = (f32[640,64]{1,0:T(8,128)S(1)}, f32[640,64]{1,0:T(8,128)S(1)}, f32[640,64]{1,0:T(8,128)S(1)}) fusion(f32[64]{0:T(128)S(1)} %multiply_power_fusion, f32[640]{0:T(1024)S(1)} %add_convert_fusion), kind=kLoop, calls=%fused_computation.4 | loop fusion | flops 81920 | bytes 494336 | tf_op jit(solution)/shard_map/neg | solution.py:487
  1.2 1.1 pad_maximum_fusion
  2.3 112.8 %shard_map.136 = bf16[640,512]{1,0:T(8,128)(2,1)} custom-call(bf16[640,256]{1,0:T(8,128)(2,1)} %q_any.1, bf16[640,256]{1,0:T(8,128)(2,1)} %k_ref.1, bf16[640,256]{1,0:T(8,128)(2,1)} %v_ref.1, bf16[640,256]{1,0:T(8,128)(2,1)} %g_any.1, f32[2,640]{1,0:T(2,128)} %ld_ref.1, f32[640,128]{1,0:T(8,128)} %get-tuple-element.8.cos_ref, ...), custom_call_target="tpu_custom_call" | custom-call | tf_op jit(solution)/shard_map/pallas_call | solution.py:498
  115.1 2.0 %copy.16 = bf16[640,512]{1,0:T(8,128)(2,1)} copy(bf16[640,512]{1,0:T(8,128)(2,1)} %shard_map.136) | data formatting | bytes 1310720
  (2 shorter events, 0.0 us)

commit v3 on v2

--- a/solution.py
+++ b/solution.py
@@ -20,9 +20,19 @@
 F32 = jnp.float32
 BF16 = jnp.bfloat16
 MSG = 144
-NSEM = 240
+NSEM = 300
 SIZE = {"sp_0": 8, "sp_1": 4, "sp_2": 2, "tp": 4}
 MARGIN = 0.3
+LOOK = 2.0
+AHEAD = 1
+DOWN_AT = 0
+EXPAND_AHEAD = 1
+ZY, YZ = ("sp_0", "sp_1"), ("sp_1", "sp_0")
+ROUTES = (
+    ((0, 1024, ZY), (1024, 1408, YZ)),
+    ((0, 768, ZY), (768, 1408, YZ)),
+    ((0, 768, ZY), (768, 1408, YZ)),
+)
 CHUNKS = ((0, 384), (384, 256))
 
 
@@ -40,6 +50,7 @@
     def __init__(self, send, recv, at):
         self.send, self.recv, self.at = send, recv, at
         self.t, self.free, self.tasks, self.made, self.count = 0.0, {}, [], [], 0
+        self.waiting = {(axis, d): [] for axis in SIZE for d in (1, -1)}
 
     def copy(self, src, dst, axis, k):
         i, size = len(self.made), SIZE[axis]
@@ -75,22 +86,40 @@
         self.count += 1
         heapq.heappush(self.tasks, (ready, self.count, flights, action))
 
+    def later(self, rank, src, dst, axis, d, then):
+        self.count += 1
+        heapq.heappush(self.waiting[axis, d], (rank, self.count, src, dst, then))
+        self.flush()
+
+    def flush(self):
+        for (axis, d), queue in self.waiting.items():
+            while queue and self.free.get((axis, d), 0.0) <= self.t + LOOK:
+                _, _, src, dst, then = heapq.heappop(queue)
+                self.when([self.copy(src, dst, axis, d)], then)
+
     def pump(self, until=None):
         limit = self.t if until is None else until
+        self.flush()
         while self.tasks and self.tasks[0][0] <= limit:
             ready, _, flights, action = heapq.heappop(self.tasks)
             self.t = max(self.t, ready)
             for flight in flights:
                 flight.landed()
             action()
+            self.flush()
+
+    def step(self):
+        if self.tasks:
+            self.pump(self.tasks[0][0])
+        else:
+            self.t = min(self.free[key] for key, queue in self.waiting.items() if queue)
+            self.flush()
 
     def work(self, us):
         self.t += us
         self.pump()
 
     def need(self, flights):
-        while any(f is None for f in flights):
-            self.pump(self.tasks[0][0])
         target = max(f.arrive for f in flights)
         self.pump(target)
         self.t = max(self.t, target)
@@ -124,10 +153,10 @@
 
 
 def kernel(
-    q_any, k_ref, v_ref, g_any, ld_ref, cos_ref, sin_ref, res_any, ow_ref,
-    gate_ref, up_ref, down_ref, ng_ref, nb_ref, fg_ref, fb_ref,
+    q_any, k_any, v_any, g_any, ld_ref, cosine_any, sine_any, res_any, ow_any,
+    gate_any, up_any, down_any, ng_ref, nb_ref, fg_ref, fb_ref,
     out_ref,
-    q_ref, g_ref, res_ref, ldp, w, ow, mx, qt, kt, inner, prefix, st, stp, ybuf, zbuf, ent,
+    q_ref, k_ref, v_ref, g_ref, res_ref, half_cos, half_sin, cos_ref, sin_ref, ldp, w, ow, mx, qt, kt, inner, prefix, st, stp, ybuf, zbuf, ent,
     total, settled, hidden, via_out, via_in, part_out, part_in, held_part, own_part, stat,
     local_sem, send_sem, recv_sem,
 ):
@@ -142,68 +171,91 @@
         pl.semaphore_signal(
             barrier, inc=1, device_id={axis: at[axis][k]}, device_id_type=pl.DeviceIdType.MESH
         )
-    own = (gate_ref, up_ref, down_ref)
     local = []
     for src, dst in (
-        [(own[m], w.at[m, z, y, c]) for m in range(3)]
-        + [(ow_ref, ow.at[x]), (q_any, q_ref), (g_any, g_ref), (res_any, res_ref)]
+        (gate_any, w.at[0, z, y, c]), (up_any, w.at[1, z, y, c]), (down_any, w.at[2, z, y, c]),
+        (ow_any, ow.at[x]), (k_any, k_ref), (cosine_any, half_cos), (sine_any, half_sin),
+        (v_any, v_ref), (q_any, q_ref), (g_any, g_ref), (res_any, res_ref),
     ):
         made = pltpu.make_async_copy(src, dst, local_sem.at[len(local)])
         made.start()
         local.append(made)
-
+    for made in local[:7]:
+        made.wait()
+    cosine, sine = half_cos[...], half_sin[...]
+    cos_ref[...] = jnp.concatenate([cosine, cosine], axis=1)
+    sin_ref[...] = jnp.concatenate([-sine, sine], axis=1)
+
+    pl.semaphore_wait(barrier, len(peers))
     net = Net(send_sem, recv_sem, at)
 
-    def gather(m, ax_a, ax_b, last):
+    def gather(m, span, ax_a, ax_b, last):
         la, lb = SIZE[ax_a], SIZE[ax_b]
         low, upper = pl.ds(0, 16), pl.ds(16, 16)
-        counts, far_a, far_b = [0] * lb, [], {}
+        counts, halves = [0] * lb, {-1: 0, 0: 0, la // 2: 0}
+        cut = pl.ds(span[0], span[1] - span[0])
 
         def shard(a, b):
             if ax_a == "sp_0":
-                return w.at[m, zo[a], yo[b], c]
-            return w.at[m, zo[b], yo[a], c]
+                return w.at[m, zo[a], yo[b], c, :, cut]
+            return w.at[m, zo[b], yo[a], c, :, cut]
+
+        mine = shard(0, 0)
 
         def landed(a, b):
             counts[b] += 1
             if counts[b] == la:
-                block = w.at[m, :, yo[b], c] if ax_a == "sp_0" else w.at[m, zo[b], :, c]
+                if ax_a == "sp_0":
+                    block = w.at[m, :, yo[b], c, :, cut]
+                else:
+                    block = w.at[m, zo[b], :, c, :, cut]
                 last.append(net.same(block, "sp_2", 1))
+
+        def copy(hops, src, dst, axis, d, then):
+            net.later((m // 2, -hops), src, dst, axis, d, then)
+
+        def half_landed(a):
+            halves[a] += 1
+            if halves[a] == 2:
+                landed(a, lb // 2)
 
         def along_b(a, k, d):
             b = -k * d % lb
-            if k < lb // 2 - 1:
-                net.when([net.same(shard(a, b), ax_b, d)], lambda: along_b(a, k + 1, d))
-            elif k == lb // 2 - 1:
+            ref = shard(a, b)
+            left = lb // 2 - k
+            if left > 1:
+                copy(left, ref, ref, ax_b, d, lambda: along_b(a, k + 1, d))
+            elif left == 1:
                 if a in (0, la // 2):
-                    part = shard(a, b).at[low if d > 0 else upper]
-                    far_b.setdefault(a, []).append(net.same(part, ax_b, d))
-                    if len(far_b[a]) == 2:
-                        net.when(far_b[a], lambda: landed(a, lb // 2))
+                    part = ref.at[low if d > 0 else upper]
+                    copy(left, part, part, ax_b, d, lambda: half_landed(a))
                 elif (a < la // 2) == (d > 0):
-                    net.when([net.same(shard(a, b), ax_b, d)], lambda: landed(a, lb // 2))
+                    copy(left, ref, ref, ax_b, d, lambda: landed(a, lb // 2))
             landed(a, b)
 
         def spread(a, src):
             for d in (1, -1):
-                flight = net.copy(src, shard(a, 0), ax_b, d)
-                net.when([flight], lambda d=d: along_b(a, 1, d))
+                copy(lb // 2, src, shard(a, 0), ax_b, d, lambda d=d: along_b(a, 1, d))
             landed(a, 0)
 
+        def far_landed():
+            halves[-1] += 1
+            if halves[-1] == 2:
+                spread(la // 2, shard(la // 2, 0))
+
         def along_a(k, d):
-            a = -k * d % la
-            if k < la // 2 - 1:
-                net.when([net.same(shard(a, 0), ax_a, d)], lambda: along_a(k + 1, d))
+            ref = shard(-k * d % la, 0)
+            left = la // 2 - k
+            if left > 1:
+                copy(left + lb // 2, ref, ref, ax_a, d, lambda: along_a(k + 1, d))
             else:
-                far_a.append(net.same(shard(a, 0).at[low if d > 0 else upper], ax_a, d))
-                if len(far_a) == 2:
-                    net.when(far_a, lambda: spread(la // 2, shard(la // 2, 0)))
-            spread(a, shard(a, 0))
+                part = ref.at[low if d > 0 else upper]
+                copy(left + lb // 2, part, part, ax_a, d, far_landed)
+            spread(-k * d % la, ref)
 
         for d in (1, -1):
-            flight = net.copy(own[m], shard(0, 0), ax_a, d)
-            net.when([flight], lambda d=d: along_a(1, d))
-        spread(0, own[m])
+            copy((la + lb) // 2, mine, shard(0, 0), ax_a, d, lambda d=d: along_a(1, d))
+        spread(0, mine)
 
     def gather_out(last):
         far = []
@@ -216,13 +268,32 @@
                 net.when(far, lambda: last.append(net.same(ow.at[xo[2], c], "sp_2", 1)))
 
         for d in (1, -1):
-            flight = net.copy(ow_ref.at[c], ow.at[x, c], "tp", d)
+            flight = net.copy(ow.at[x, c], ow.at[x, c], "tp", d)
             net.when([flight], lambda d=d: step(d))
 
     def all_of(flights, count):
+        if count == 0:
+            return
         while len(flights) < count:
-            net.pump(net.tasks[0][0])
+            net.step()
         net.need(flights)
+
+    arrived = [[], [], []]
+    expected = [0, 0, 0]
+
+    def start(m):
+        for lo, hi, route in ROUTES[m]:
+            gather(m, (lo, hi), *route, arrived[m])
+            expected[m] += SIZE[route[1]]
+
+    outs_in = []
+    start(0)
+    start(1)
+    if DOWN_AT == 0:
+        start(2)
+    gather_out(outs_in)
+    for made in local[7:]:
+        made.wait()
 
     cols = [pl.ds(h * HD, HD) for h in range(2)]
     rows = [pl.ds(n * BLOCK, BLOCK) for n in range(NB)]
@@ -261,16 +332,10 @@
             before[r] = so_far
             state = jnp.exp(end) * state + tn(keyed, v_ref[rows[n], cols[h]])
             so_far = so_far + end
+            net.work(0.1)
         write_message(st.at[h], state, jnp.exp(so_far))
 
-    pl.semaphore_wait(barrier, len(peers))
     core_swap = net.copy(st, stp, "sp_2", 1)
-    gates_in, ups_in, downs_in, outs_in = [], [], [], []
-    gather(0, "sp_0", "sp_1", gates_in)
-    gather(1, "sp_1", "sp_0", ups_in)
-    gather_out(outs_in)
-    for made in local:
-        made.wait()
 
     def inside(h, n):
         r = n * 2 + h
@@ -280,7 +345,7 @@
         damping = jnp.where(lower, jnp.exp(jnp.minimum(gap, 0.0)), 0.0)
         weights = (nt(query, kt[rows[n], cols[h]]) * damping).astype(BF16)
         inner[rows[n], cols[h]] = nn(weights, v_ref[rows[n], cols[h]])
-        net.work(0.4)
+        net.work(0.1)
 
     inside(0, 0)
     inside(0, 1)
@@ -292,6 +357,8 @@
     d1 = jnp.where(first, peer_d, mine_d)
     write_message(ybuf.at[0], d1 * s0 + s1, mine_d * peer_d)
     y_sends = [net.copy(ybuf.at[0], ybuf.at[k], "sp_1", k) for k in (1, 3, 2)]
+    if DOWN_AT == 1:
+        start(2)
     for n in range(2, NB):
         inside(0, n)
     inside(1, 0)
@@ -312,13 +379,16 @@
     ahead_y, decay_y, plane, plane_decay = running(ybuf, 4, y)
     write_message(zbuf.at[0], plane, plane_decay)
     z_sends = [net.copy(zbuf.at[0], zbuf.at[k], "sp_0", k) for k in (1, 7, 2, 6, 3, 5, 4)]
+    if DOWN_AT == 2:
+        start(2)
     for n in range(2, NB):
         inside(1, n)
     net.need(z_sends)
     ahead_z = running(zbuf, 8, z)[0]
     ent[c] = decay_y * ahead_z + ahead_y
     ent_swap = net.same(ent.at[c], "sp_2", 1)
-    gather(2, "sp_0", "sp_1", downs_in)
+    if DOWN_AT == 3:
+        start(2)
     net.need([ent_swap])
     entering = []
     for h in range(2):
@@ -346,7 +416,7 @@
         block = mx.at[rows[n], pl.ds(pl.multiple_of(x * 256, 256), 256)]
         for d in (1, -1):
             net.when([net.same(block, "tp", d)], lambda n=n, d=d: mixed_step(n, d))
-        net.work(0.6)
+        net.work(0.15)
 
     def project(lo, size):
         for part in range(2):
@@ -357,7 +427,7 @@
                 mix = nn(mx[lo : lo + size], ow[:, :, :, span].reshape(1024, 256))
                 total[lo : lo + size, span] = ALPHA * res_ref[lo : lo + size, span].astype(F32) + mix
 
-            net.work(0.0045 * size)
+            net.work(0.0033 * size)
 
         @pl.loop(lo // 32, (lo + size) // 32)
         def _(i):
@@ -368,7 +438,7 @@
             scaled = center * lax.rsqrt(spread + EPS)
             settled[span] = (scaled * ng_ref[...] + nb_ref[...]).astype(BF16)
 
-        net.work(0.004 * size)
+        net.work(0.003 * size)
 
     def expand(lo, size):
         for j in range(6):
@@ -378,7 +448,7 @@
             gate = nn(acts, w[0, :, :, :, :, span].reshape(2048, width))
             lift = nn(acts, w[1, :, :, :, :, span].reshape(2048, width))
             hidden[lo : lo + size, span] = (gate / (1.0 + jnp.exp(-gate)) * lift).astype(BF16)
-            net.work(0.0043 * size)
+            net.work(0.0038 * size)
 
     own_cols = pl.ds(pl.multiple_of(x * 512, 512), 512)
     last_sums = []
@@ -390,7 +460,7 @@
         def part(span, dest):
             acts = hidden[span[0] : span[1]]
             value = nt(acts, w[2, pl.ds(2 * dest, 2)].reshape(512, 1408))
-            net.t += 0.003 * half
+            net.t += 0.0025 * half
             return value
 
         def at_(ref, k, span):
@@ -434,7 +504,7 @@
             both = jnp.where(lane == 0, s, jnp.where(lane == 1, q, 0.0))
             stat[0, n] = both.T[0:8]
         span = pl.ds(lo // BLOCK, size // BLOCK)
-        net.work(0.004 * size)
+        net.work(0.002 * size)
         return [net.copy(stat.at[0, span], stat.at[k, span], "tp", k) for k in (1, 3, 2)]
 
     def settle(lo, size, stats):
@@ -447,29 +517,36 @@
             spread = wide[:, 1:2] / 2048.0 - mean * mean
             scaled = (own_part[a:b] - mean) * lax.rsqrt(spread + EPS)
             out_ref[a:b] = (scaled * fg_ref[:, own_cols] + fb_ref[:, own_cols]).astype(BF16)
-        net.work(0.004 * size)
+        net.work(0.002 * size)
 
     def mixed_ready(lo, size):
         for n in range(lo // BLOCK, (lo + size) // BLOCK):
             all_of(mixed_in[n], 2)
 
     all_of(outs_in, 3)
-    mixed_ready(*CHUNKS[0])
-    project(*CHUNKS[0])
-    all_of(gates_in, 4)
-    all_of(ups_in, 8)
-    expand(*CHUNKS[0])
-    mixed_ready(*CHUNKS[1])
-    project(*CHUNKS[1])
-    all_of(downs_in, 4)
-    sums_0 = contract(*CHUNKS[0])
-    expand(*CHUNKS[1])
-    sums_1 = contract(*CHUNKS[1])
-    stats_0 = sum_up(*CHUNKS[0], sums_0)
-    settle(*CHUNKS[0], stats_0)
-    stats_1 = sum_up(*CHUNKS[1], sums_1)
-    settle(*CHUNKS[1], stats_1)
-    assert not net.tasks
+    sums, stats = [], []
+    done = grown = 0
+    for i, chunk in enumerate(CHUNKS):
+        while grown < min(len(CHUNKS), i + EXPAND_AHEAD):
+            while done < min(len(CHUNKS), grown + AHEAD):
+                mixed_ready(*CHUNKS[done])
+                project(*CHUNKS[done])
+                done += 1
+            if grown == 0:
+                all_of(arrived[0], expected[0])
+                all_of(arrived[1], expected[1])
+            expand(*CHUNKS[grown])
+            grown += 1
+        if i == 0:
+            all_of(arrived[2], expected[2])
+        sums.append(contract(*chunk))
+        if i >= 2:
+            stats.append(sum_up(*CHUNKS[i - 2], sums[i - 2]))
+    for i in range(len(CHUNKS)):
+        if i >= len(stats):
+            stats.append(sum_up(*CHUNKS[i], sums[i]))
+        settle(*CHUNKS[i], stats[i])
+    assert not net.tasks and not any(net.waiting.values())
     for flight in net.made:
         flight.made.wait_send()
 
@@ -483,15 +560,13 @@
     freqs = ROPE_BASE ** (-2.0 * jnp.arange(64, dtype=F32) / HD)
     angles = positions[:, None] * freqs[None, :]
     cosine, sine = jnp.cos(angles), jnp.sin(angles)
-    cosines = jnp.concatenate([cosine, cosine], axis=1)
-    sines = jnp.concatenate([-sine, sine], axis=1)
     args = (
-        queries, key_input, value_input, gate_input, log_decay, cosines, sines, residual,
+        queries, key_input, value_input, gate_input, log_decay, cosine, sine, residual,
         out_weight.reshape(2, 128, 2048), gate_weight, up_weight, down_weight.T,
         norm_gain[None], norm_bias[None], final_gain[None], final_bias[None],
     )
     vm = pltpu.VMEM
-    late = (0, 3, 7)
+    late = (0, 1, 2, 3, 5, 6, 7, 8, 9, 10, 11)
     placed = [
         pl.BlockSpec(memory_space=pl.ANY if i in late else vm) for i in range(len(args))
     ]
@@ -503,7 +578,13 @@
         scratch_shapes=[
             vm((ROWS, 256), BF16),
             vm((ROWS, 256), BF16),
+            vm((ROWS, 256), BF16),
+            vm((ROWS, 256), BF16),
             vm((ROWS, 2048), BF16),
+            vm((ROWS, HD // 2), F32),
+            vm((ROWS, HD // 2), F32),
+            vm((ROWS, HD), F32),
+            vm((ROWS, HD), F32),
             vm((16, BLOCK), F32),
             vm((3, 8, 4, 2, 32, 1408), BF16),
             vm((4, 2, 128, 2048), BF16),
@@ -527,7 +608,7 @@
             vm((ROWS, 512), F32),
             vm((ROWS, 512), F32),
             vm((4, NB, 8, 128), F32),
-            pltpu.SemaphoreType.DMA((7,)),
+            pltpu.SemaphoreType.DMA((11,)),
             pltpu.SemaphoreType.DMA((NSEM,)),
             pltpu.SemaphoreType.DMA((NSEM,)),
         ],

time: 117 us -> 112 us (0.957)
  Pallas kernels: 113 us -> 108 us
    pallas_call x1, Pallas kernels: 113 us -> 108 us  [shards(): pl.pallas_call(kernel, out_shape=jax.ShapeDtypeStruct((ROWS, 512), BF16),...]
    sin x0 -> x1, other arithmetic: none -> 2.06 us  [shards(): cosine, sine = (jnp.cos(angles), jnp.sin(angles))]
    neg x1 -> x0, other arithmetic: 1.22 us -> none  [shards(): sines = jnp.concatenate([-sine, sine], axis=1)]
where the time goes in v3:
time: 112 us
  Pallas kernels  108 us (96%)
  other arithmetic  2.08 us (2%)
  local copies, waits for them, and re-layouts  1.97 us (2%)
    pallas_call x1, Pallas kernels, shards(): pl.pallas_call(kernel, out_shape=jax.ShapeDtypeStruct((ROWS, 512), BF16),...  108 us

profile of v3, /device:TPU:1, one launch (start us, length us, event | category | flops | bytes accessed | tf_op | source)
XLA Modules:
  0.0 112.1 jit_solution(4938530679305669812)
XLA Ops:
  0.0 2.1 %multiply_sine_fusion = (f32[640,64]{1,0:T(8,128)}, f32[640,64]{1,0:T(8,128)}) fusion(f32[64]{0:T(128)S(1)} %multiply_power_fusion, f32[640]{0:T(1024)S(1)} %add_convert_fusion), kind=kLoop, calls=%fused_computation | loop fusion | flops 40960 | bytes 330496 | tf_op jit(solution)/shard_map/sin | solution.py:562
  2.1 108.1 %shard_map.136 = bf16[640,512]{1,0:T(8,128)(2,1)} custom-call(bf16[640,256]{1,0:T(8,128)(2,1)} %q_any.1, bf16[640,256]{1,0:T(8,128)(2,1)} %k_any.1, bf16[640,256]{1,0:T(8,128)(2,1)} %v_any.1, bf16[640,256]{1,0:T(8,128)(2,1)} %g_any.1, f32[2,640]{1,0:T(2,128)} %ld_ref.1, f32[640,64]{1,0:T(8,128)} %get-tuple-element.6.cosine_any, ...), custom_call_target="tpu_custom_call" | custom-call | tf_op jit(solution)/shard_map/pallas_call | solution.py:573
  110.2 2.0 %copy.16 = bf16[640,512]{1,0:T(8,128)(2,1)} copy(bf16[640,512]{1,0:T(8,128)(2,1)} %shard_map.136) | data formatting | bytes 1310720
  (2 shorter events, 0.0 us)

commit v4 on v3

--- a/solution.py
+++ b/solution.py
@@ -3,6 +3,7 @@
 
 import jax
 import jax.numpy as jnp
+import numpy as np
 from jax import lax
 from jax.experimental import pallas as pl
 from jax.experimental.pallas import tpu as pltpu
@@ -20,7 +21,8 @@
 F32 = jnp.float32
 BF16 = jnp.bfloat16
 MSG = 144
-NSEM = 300
+NSEM = 190
+POOL = 48
 SIZE = {"sp_0": 8, "sp_1": 4, "sp_2": 2, "tp": 4}
 MARGIN = 0.3
 LOOK = 2.0
@@ -29,8 +31,8 @@
 EXPAND_AHEAD = 1
 ZY, YZ = ("sp_0", "sp_1"), ("sp_1", "sp_0")
 ROUTES = (
-    ((0, 1024, ZY), (1024, 1408, YZ)),
-    ((0, 768, ZY), (768, 1408, YZ)),
+    ((0, 1408, ZY),),
+    ((0, 640, ZY), (640, 1408, YZ)),
     ((0, 768, ZY), (768, 1408, YZ)),
 )
 CHUNKS = ((0, 384), (384, 256))
@@ -46,23 +48,53 @@
             self.open = False
 
 
+class Group:
+    def __init__(self, net, total, count):
+        self.net, self.total, self.count = net, total, count
+        self.index = net.take()
+        self.flights, self.arrive, self.open = [], 0.0, True
+
+    def add(self, flight):
+        self.flights.append(flight)
+        self.arrive = max(self.arrive, flight.arrive)
+        return len(self.flights) == self.count
+
+    def landed(self):
+        assert len(self.flights) == self.count
+        if self.open:
+            self.net.describe(self.total, self.total, 0, self.index, "sp_2", 1).wait_recv()
+            self.open = False
+
+
 class Net:
     def __init__(self, send, recv, at):
         self.send, self.recv, self.at = send, recv, at
         self.t, self.free, self.tasks, self.made, self.count = 0.0, {}, [], [], 0
+        self.taken = 0
         self.waiting = {(axis, d): [] for axis in SIZE for d in (1, -1)}
 
-    def copy(self, src, dst, axis, k):
-        i, size = len(self.made), SIZE[axis]
-        k %= size
-        made = pltpu.make_async_remote_copy(
+    def take(self):
+        self.taken += 1
+        return self.taken - 1
+
+    def describe(self, src, dst, send, recv, axis, k):
+        return pltpu.make_async_remote_copy(
             src_ref=src,
             dst_ref=dst,
-            send_sem=self.send.at[i],
-            recv_sem=self.recv.at[i],
+            send_sem=self.send.at[send],
+            recv_sem=self.recv.at[recv],
             device_id={axis: self.at[axis][k]},
             device_id_type=pl.DeviceIdType.MESH,
         )
+
+    def copy(self, src, dst, axis, k, group=None):
+        size = SIZE[axis]
+        k %= size
+        i = len(self.made)
+        if i >= POOL:
+            self.made[i - POOL].made.wait_send()
+        recv = self.take() if group is None else group.index
+        made = self.describe(src, dst, i % POOL, recv, axis, k)
         made.start()
         nbytes = math.prod(src.shape) * src.dtype.itemsize
         hops = min(k, size - k)
@@ -78,24 +110,28 @@
         self.made.append(flight)
         return flight
 
-    def same(self, ref, axis, k):
-        return self.copy(ref, ref, axis, k)
+    def same(self, ref, axis, k, group=None):
+        return self.copy(ref, ref, axis, k, group)
 
     def when(self, flights, action):
         ready = max(f.arrive for f in flights) + MARGIN
         self.count += 1
         heapq.heappush(self.tasks, (ready, self.count, flights, action))
 
-    def later(self, rank, src, dst, axis, d, then):
+    def later(self, rank, src, dst, axis, d, then, group=None):
         self.count += 1
-        heapq.heappush(self.waiting[axis, d], (rank, self.count, src, dst, then))
+        heapq.heappush(self.waiting[axis, d], (rank, self.count, src, dst, then, group))
         self.flush()
 
     def flush(self):
         for (axis, d), queue in self.waiting.items():
             while queue and self.free.get((axis, d), 0.0) <= self.t + LOOK:
-                _, _, src, dst, then = heapq.heappop(queue)
-                self.when([self.copy(src, dst, axis, d)], then)
+                _, _, src, dst, then, group = heapq.heappop(queue)
+                flight = self.copy(src, dst, axis, d, group)
+                if group is None:
+                    self.when([flight], then)
+                elif group.add(flight):
+                    self.when([group], then)
 
     def pump(self, until=None):
         limit = self.t if until is None else until
@@ -153,10 +189,10 @@
 
 
 def kernel(
-    q_any, k_any, v_any, g_any, ld_ref, cosine_any, sine_any, res_any, ow_any,
+    q_any, k_any, v_any, g_any, ld_ref, freq_ref, res_any, ow_any,
     gate_any, up_any, down_any, ng_ref, nb_ref, fg_ref, fb_ref,
     out_ref,
-    q_ref, k_ref, v_ref, g_ref, res_ref, half_cos, half_sin, cos_ref, sin_ref, ldp, w, ow, mx, qt, kt, inner, prefix, st, stp, ybuf, zbuf, ent,
+    q_ref, k_ref, v_ref, g_ref, res_ref, cos_ref, sin_ref, ldp, w, ow, mx, qt, kt, inner, prefix, st, stp, ybuf, zbuf, ent,
     total, settled, hidden, via_out, via_in, part_out, part_in, held_part, own_part, stat,
     local_sem, send_sem, recv_sem,
 ):
@@ -174,25 +210,21 @@
     local = []
     for src, dst in (
         (gate_any, w.at[0, z, y, c]), (up_any, w.at[1, z, y, c]), (down_any, w.at[2, z, y, c]),
-        (ow_any, ow.at[x]), (k_any, k_ref), (cosine_any, half_cos), (sine_any, half_sin),
+        (ow_any, ow.at[x]), (k_any, k_ref),
         (v_any, v_ref), (q_any, q_ref), (g_any, g_ref), (res_any, res_ref),
     ):
         made = pltpu.make_async_copy(src, dst, local_sem.at[len(local)])
         made.start()
         local.append(made)
-    for made in local[:7]:
+    for made in local[:4]:
         made.wait()
-    cosine, sine = half_cos[...], half_sin[...]
-    cos_ref[...] = jnp.concatenate([cosine, cosine], axis=1)
-    sin_ref[...] = jnp.concatenate([-sine, sine], axis=1)
-
     pl.semaphore_wait(barrier, len(peers))
     net = Net(send_sem, recv_sem, at)
 
     def gather(m, span, ax_a, ax_b, last):
         la, lb = SIZE[ax_a], SIZE[ax_b]
         low, upper = pl.ds(0, 16), pl.ds(16, 16)
-        counts, halves = [0] * lb, {-1: 0, 0: 0, la // 2: 0}
+        counts, halves = [0] * lb, [0]
         cut = pl.ds(span[0], span[1] - span[0])
 
         def shard(a, b):
@@ -202,22 +234,26 @@
 
         mine = shard(0, 0)
 
+        def block(b):
+            if ax_a == "sp_0":
+                return w.at[m, :, yo[b], c, :, cut]
+            return w.at[m, zo[b], :, c, :, cut]
+
+        def hand_over(b):
+            last.add(net.same(block(b), "sp_2", 1, last))
+
         def landed(a, b):
             counts[b] += 1
             if counts[b] == la:
-                if ax_a == "sp_0":
-                    block = w.at[m, :, yo[b], c, :, cut]
-                else:
-                    block = w.at[m, zo[b], :, c, :, cut]
-                last.append(net.same(block, "sp_2", 1))
-
-        def copy(hops, src, dst, axis, d, then):
-            net.later((m // 2, -hops), src, dst, axis, d, then)
-
-        def half_landed(a):
-            halves[a] += 1
-            if halves[a] == 2:
-                landed(a, lb // 2)
+                hand_over(b)
+
+        far = Group(net, block(lb // 2), la + 2)
+
+        def copy(hops, src, dst, axis, d, then, group=None):
+            net.later((m // 2, -hops), src, dst, axis, d, then, group)
+
+        def far_full():
+            hand_over(lb // 2)
 
         def along_b(a, k, d):
             b = -k * d % lb
@@ -228,9 +264,9 @@
             elif left == 1:
                 if a in (0, la // 2):
                     part = ref.at[low if d > 0 else upper]
-                    copy(left, part, part, ax_b, d, lambda: half_landed(a))
+                    copy(left, part, part, ax_b, d, far_full, far)
                 elif (a < la // 2) == (d > 0):
-                    copy(left, ref, ref, ax_b, d, lambda: landed(a, lb // 2))
+                    copy(left, ref, ref, ax_b, d, far_full, far)
             landed(a, b)
 
         def spread(a, src):
@@ -239,8 +275,8 @@
             landed(a, 0)
 
         def far_landed():
-            halves[-1] += 1
-            if halves[-1] == 2:
+            halves[0] += 1
+            if halves[0] == 2:
                 spread(la // 2, shard(la // 2, 0))
 
         def along_a(k, d):
@@ -278,13 +314,19 @@
             net.step()
         net.need(flights)
 
-    arrived = [[], [], []]
-    expected = [0, 0, 0]
+    arrived = [
+        Group(net, w.at[m, :, :, 1 - c], sum(SIZE[route[1]] for _, _, route in ROUTES[m]))
+        for m in range(3)
+    ]
 
     def start(m):
         for lo, hi, route in ROUTES[m]:
             gather(m, (lo, hi), *route, arrived[m])
-            expected[m] += SIZE[route[1]]
+
+    def whole(group):
+        while len(group.flights) < group.count:
+            net.step()
+        net.need([group])
 
     outs_in = []
     start(0)
@@ -292,8 +334,15 @@
     if DOWN_AT == 0:
         start(2)
     gather_out(outs_in)
-    for made in local[7:]:
+    for made in local[4:]:
         made.wait()
+
+    at_position = lax.broadcasted_iota(jnp.int32, (ROWS, HD // 2), 0) + ((z * 4 + y) * 2 + c) * ROWS
+    angles = at_position.astype(F32) * freq_ref[...]
+    cosine, sine = jnp.cos(angles), jnp.sin(angles)
+    cos_ref[...] = jnp.concatenate([cosine, cosine], axis=1)
+    sin_ref[...] = jnp.concatenate([-sine, sine], axis=1)
+    net.work(2.3)
 
     cols = [pl.ds(h * HD, HD) for h in range(2)]
     rows = [pl.ds(n * BLOCK, BLOCK) for n in range(NB)]
@@ -395,12 +444,13 @@
         s, d = read_message(stp.at[h])
         entering.append(jnp.where(c == 1, d * ent[h] + s, ent[h]))
 
-    mixed_in = [[] for _ in range(NB)]
+    far_cols = pl.ds(pl.multiple_of(xo[2] * 256, 256), 256)
+    mixed_in = [Group(net, mx.at[rows[n], far_cols], 2) for n in range(NB)]
 
     def mixed_step(n, d):
         start = n * BLOCK + (0 if d > 0 else 64)
         where = pl.ds(pl.multiple_of(xo[-d % 4] * 256, 256), 256)
-        mixed_in[n].append(net.same(mx.at[pl.ds(start, 64), where], "tp", d))
+        mixed_in[n].add(net.same(mx.at[pl.ds(start, 64), where], "tp", d, mixed_in[n]))
 
     for n in range(NB):
         for h in range(2):
@@ -521,7 +571,7 @@
 
     def mixed_ready(lo, size):
         for n in range(lo // BLOCK, (lo + size) // BLOCK):
-            all_of(mixed_in[n], 2)
+            whole(mixed_in[n])
 
     all_of(outs_in, 3)
     sums, stats = [], []
@@ -533,12 +583,12 @@
                 project(*CHUNKS[done])
                 done += 1
             if grown == 0:
-                all_of(arrived[0], expected[0])
-                all_of(arrived[1], expected[1])
+                whole(arrived[0])
+                whole(arrived[1])
             expand(*CHUNKS[grown])
             grown += 1
         if i == 0:
-            all_of(arrived[2], expected[2])
+            whole(arrived[2])
         sums.append(contract(*chunk))
         if i >= 2:
             stats.append(sum_up(*CHUNKS[i - 2], sums[i - 2]))
@@ -547,7 +597,7 @@
             stats.append(sum_up(*CHUNKS[i], sums[i]))
         settle(*CHUNKS[i], stats[i])
     assert not net.tasks and not any(net.waiting.values())
-    for flight in net.made:
+    for flight in net.made[-POOL:]:
         flight.made.wait_send()
 
 
@@ -555,18 +605,14 @@
     queries, key_input, value_input, gate_input, log_decay, residual, out_weight,
     norm_gain, norm_bias, gate_weight, up_weight, down_weight, final_gain, final_bias,
 ):
-    offset = lax.axis_index(SP) * ROWS
-    positions = (offset + jnp.arange(ROWS, dtype=jnp.int32)).astype(F32)
-    freqs = ROPE_BASE ** (-2.0 * jnp.arange(64, dtype=F32) / HD)
-    angles = positions[:, None] * freqs[None, :]
-    cosine, sine = jnp.cos(angles), jnp.sin(angles)
+    freqs = (ROPE_BASE ** (-2.0 * np.arange(HD // 2) / HD)).astype(np.float32)[None]
     args = (
-        queries, key_input, value_input, gate_input, log_decay, cosine, sine, residual,
+        queries, key_input, value_input, gate_input, log_decay, freqs, residual,
         out_weight.reshape(2, 128, 2048), gate_weight, up_weight, down_weight.T,
         norm_gain[None], norm_bias[None], final_gain[None], final_bias[None],
     )
     vm = pltpu.VMEM
-    late = (0, 1, 2, 3, 5, 6, 7, 8, 9, 10, 11)
+    late = (0, 1, 2, 3, 6, 7, 8, 9, 10)
     placed = [
         pl.BlockSpec(memory_space=pl.ANY if i in late else vm) for i in range(len(args))
     ]
@@ -581,8 +627,6 @@
             vm((ROWS, 256), BF16),
             vm((ROWS, 256), BF16),
             vm((ROWS, 2048), BF16),
-            vm((ROWS, HD // 2), F32),
-            vm((ROWS, HD // 2), F32),
             vm((ROWS, HD), F32),
             vm((ROWS, HD), F32),
             vm((16, BLOCK), F32),
@@ -608,8 +652,8 @@
             vm((ROWS, 512), F32),
             vm((ROWS, 512), F32),
             vm((4, NB, 8, 128), F32),
-            pltpu.SemaphoreType.DMA((11,)),
-            pltpu.SemaphoreType.DMA((NSEM,)),
+            pltpu.SemaphoreType.DMA((9,)),
+            pltpu.SemaphoreType.DMA((POOL,)),
             pltpu.SemaphoreType.DMA((NSEM,)),
         ],
         compiler_params=pltpu.CompilerParams(

time: 112 us -> 105 us (0.938)
  Pallas kernels: 108 us -> 103 us
  other arithmetic: 2.08 us -> 0 us
    pallas_call x1, Pallas kernels: 108 us -> 103 us  [shards(): pl.pallas_call(kernel, out_shape=jax.ShapeDtypeStruct((ROWS, 512), BF16),...]
    sin x1 -> x0, other arithmetic: 2.06 us -> none  [shards(): cosine, sine = (jnp.cos(angles), jnp.sin(angles))]
where the time goes in v4:
time: 105 us
  Pallas kernels  103 us (98%)
  local copies, waits for them, and re-layouts  1.97 us (2%)
    pallas_call x1, Pallas kernels, shards(): pl.pallas_call(kernel, out_shape=jax.ShapeDtypeStruct((ROWS, 512), BF16),...  103 us

profile of v4, /device:TPU:1, one launch (start us, length us, event | category | flops | bytes accessed | tf_op | source)
XLA Modules:
  0.0 105.0 jit_solution(444630886496938771)
XLA Ops:
  0.0 103.1 %shard_map.145 = bf16[640,512]{1,0:T(8,128)(2,1)} custom-call(bf16[640,256]{1,0:T(8,128)(2,1)} %q_any.1, bf16[640,256]{1,0:T(8,128)(2,1)} %k_any.1, bf16[640,256]{1,0:T(8,128)(2,1)} %v_any.1, bf16[640,256]{1,0:T(8,128)(2,1)} %g_any.1, f32[2,640]{1,0:T(2,128)} %ld_ref.1, f32[1,64]{1,0:T(1,128)} %constant.2.clone.freq_ref, bf16[640,2048]{1,0:T(8,128)(2,1)} %res_any.1, ...), custom_call_target="tpu_custom_call" | custom-call | tf_op jit(solution)/shard_map/pallas_call | solution.py:619
  103.1 2.0 %copy.17 = bf16[640,512]{1,0:T(8,128)(2,1)} copy(bf16[640,512]{1,0:T(8,128)(2,1)} %shard_map.145) | data formatting | bytes 1310720

commit v5 on v4

--- a/solution.py
+++ b/solution.py
@@ -21,18 +21,18 @@
 F32 = jnp.float32
 BF16 = jnp.bfloat16
 MSG = 144
-NSEM = 190
+NSEM = 194
 POOL = 48
 SIZE = {"sp_0": 8, "sp_1": 4, "sp_2": 2, "tp": 4}
-MARGIN = 0.3
-LOOK = 2.0
+MARGIN = 0.0
+LOOK = 1.5
 AHEAD = 1
 DOWN_AT = 0
 EXPAND_AHEAD = 1
 ZY, YZ = ("sp_0", "sp_1"), ("sp_1", "sp_0")
 ROUTES = (
     ((0, 1408, ZY),),
-    ((0, 640, ZY), (640, 1408, YZ)),
+    ((0, 384, ZY), (384, 1408, YZ)),
     ((0, 768, ZY), (768, 1408, YZ)),
 )
 CHUNKS = ((0, 384), (384, 256))
@@ -176,23 +176,25 @@
 
 
 def write_message(ref, state, decay):
-    ref[0:HD] = state.astype(BF16)
+    size = state.shape[0]
+    ref[0:size] = state.astype(BF16)
     high = jnp.broadcast_to(decay, (16, HD)).astype(BF16).astype(F32)
     row = lax.broadcasted_iota(jnp.int32, (16, HD), 0)
     rest = jnp.broadcast_to(decay, (16, HD)) - high
-    ref[HD:MSG] = jnp.where(row == 0, high, jnp.where(row == 1, rest, 0.0)).astype(BF16)
+    ref[size : size + 16] = jnp.where(row == 0, high, jnp.where(row == 1, rest, 0.0)).astype(BF16)
 
 
 def read_message(ref):
-    tail = ref[HD:MSG].astype(F32)
-    return ref[0:HD].astype(F32), tail[0:1] + tail[1:2]
+    size = ref.shape[0] - 16
+    tail = ref[size : size + 16].astype(F32)
+    return ref[0:size].astype(F32), tail[0:1] + tail[1:2]
 
 
 def kernel(
     q_any, k_any, v_any, g_any, ld_ref, freq_ref, res_any, ow_any,
     gate_any, up_any, down_any, ng_ref, nb_ref, fg_ref, fb_ref,
     out_ref,
-    q_ref, k_ref, v_ref, g_ref, res_ref, cos_ref, sin_ref, ldp, w, ow, mx, qt, kt, inner, prefix, st, stp, ybuf, zbuf, ent,
+    q_ref, k_ref, v_ref, g_ref, res_ref, cos_ref, sin_ref, ldp, w, ow, mx, qt, kt, inner, prefix, st, stp, ybuf, zbuf, plane_ref, ahead_ref, ent,
     total, settled, hidden, via_out, via_in, part_out, part_in, held_part, own_part, stat,
     local_sem, send_sem, recv_sem,
 ):
@@ -414,7 +416,7 @@
     inside(1, 1)
 
     def running(buf, count, place):
-        run, decay = jnp.zeros((HD, HD), F32), jnp.ones((1, HD), F32)
+        run, decay = jnp.zeros((buf.shape[1] - 16, HD), F32), jnp.ones((1, HD), F32)
         ahead, ahead_decay = run, decay
         for i in range(count):
             passed = i == place
@@ -426,15 +428,19 @@
 
     net.need(y_sends)
     ahead_y, decay_y, plane, plane_decay = running(ybuf, 4, y)
-    write_message(zbuf.at[0], plane, plane_decay)
+    plane_ref[...] = plane
+    quarter = pl.ds(pl.multiple_of(y * 32, 32), 32)
+    write_message(zbuf.at[0], plane_ref[quarter], plane_decay)
     z_sends = [net.copy(zbuf.at[0], zbuf.at[k], "sp_0", k) for k in (1, 7, 2, 6, 3, 5, 4)]
     if DOWN_AT == 2:
         start(2)
     for n in range(2, NB):
         inside(1, n)
     net.need(z_sends)
-    ahead_z = running(zbuf, 8, z)[0]
-    ent[c] = decay_y * ahead_z + ahead_y
+    ahead_ref[quarter] = running(zbuf, 8, z)[0]
+    joins = [net.same(ahead_ref.at[quarter], "sp_1", k) for k in (1, 3, 2)]
+    net.need(joins)
+    ent[c] = decay_y * ahead_ref[...] + ahead_y
     ent_swap = net.same(ent.at[c], "sp_2", 1)
     if DOWN_AT == 3:
         start(2)
@@ -596,6 +602,7 @@
         if i >= len(stats):
             stats.append(sum_up(*CHUNKS[i], sums[i]))
         settle(*CHUNKS[i], stats[i])
+    assert net.taken <= NSEM
     assert not net.tasks and not any(net.waiting.values())
     for flight in net.made[-POOL:]:
         flight.made.wait_send()
@@ -640,7 +647,9 @@
             vm((2, MSG, HD), BF16),
             vm((2, MSG, HD), BF16),
             vm((4, MSG, HD), BF16),
-            vm((8, MSG, HD), BF16),
+            vm((8, 48, HD), BF16),
+            vm((HD, HD), F32),
+            vm((HD, HD), F32),
             vm((2, HD, HD), F32),
             vm((ROWS, 2048), F32),
             vm((ROWS, 2048), BF16),

time: 105 us -> 106 us (level)
  no operation moved by 1% of the time
where the time goes in v5:
time: 106 us; the launch traced here: 105 us
  Pallas kernels  103 us (97%)
  local copies, waits for them, and re-layouts  1.97 us (2%)
    pallas_call x1, Pallas kernels, shards(): pl.pallas_call(kernel, out_shape=jax.ShapeDtypeStruct((ROWS, 512), BF16),...  103 us

profile of v5, /device:TPU:1, one launch (start us, length us, event | category | flops | bytes accessed | tf_op | source)
XLA Modules:
  0.0 105.4 jit_solution(12882436422669255181)
XLA Ops:
  0.0 103.5 %shard_map.145 = bf16[640,512]{1,0:T(8,128)(2,1)} custom-call(bf16[640,256]{1,0:T(8,128)(2,1)} %q_any.1, bf16[640,256]{1,0:T(8,128)(2,1)} %k_any.1, bf16[640,256]{1,0:T(8,128)(2,1)} %v_any.1, bf16[640,256]{1,0:T(8,128)(2,1)} %g_any.1, f32[2,640]{1,0:T(2,128)} %ld_ref.1, f32[1,64]{1,0:T(1,128)} %constant.2.clone.freq_ref, bf16[640,2048]{1,0:T(8,128)(2,1)} %res_any.1, ...), custom_call_target="tpu_custom_call" | custom-call | tf_op jit(solution)/shard_map/pallas_call | solution.py:626
  103.5 2.0 %copy.17 = bf16[640,512]{1,0:T(8,128)(2,1)} copy(bf16[640,512]{1,0:T(8,128)(2,1)} %shard_map.145) | data formatting | bytes 1310720

commit v6 on v5

--- a/solution.py
+++ b/solution.py
@@ -24,15 +24,15 @@
 NSEM = 194
 POOL = 48
 SIZE = {"sp_0": 8, "sp_1": 4, "sp_2": 2, "tp": 4}
-MARGIN = 0.0
-LOOK = 1.5
+MARGIN = 0.3
+LOOK = 3.0
 AHEAD = 1
 DOWN_AT = 0
 EXPAND_AHEAD = 1
 ZY, YZ = ("sp_0", "sp_1"), ("sp_1", "sp_0")
 ROUTES = (
     ((0, 1408, ZY),),
-    ((0, 384, ZY), (384, 1408, YZ)),
+    ((0, 640, ZY), (640, 1408, YZ)),
     ((0, 768, ZY), (768, 1408, YZ)),
 )
 CHUNKS = ((0, 384), (384, 256))

time: 106 us -> 104 us (0.981)
    pallas_call x1, Pallas kernels: 103 us -> 102 us  [shards(): pl.pallas_call(kernel, out_shape=jax.ShapeDtypeStruct((ROWS, 512), BF16),...]
where the time goes in v6:
time: 104 us
  Pallas kernels  102 us (98%)
  local copies, waits for them, and re-layouts  1.97 us (2%)
    pallas_call x1, Pallas kernels, shards(): pl.pallas_call(kernel, out_shape=jax.ShapeDtypeStruct((ROWS, 512), BF16),...  102 us

profile of v6, /device:TPU:1, one launch (start us, length us, event | category | flops | bytes accessed | tf_op | source)
XLA Modules:
  0.0 104.2 jit_solution(587087835025582293)
XLA Ops:
  0.0 102.2 %shard_map.145 = bf16[640,512]{1,0:T(8,128)(2,1)} custom-call(bf16[640,256]{1,0:T(8,128)(2,1)} %q_any.1, bf16[640,256]{1,0:T(8,128)(2,1)} %k_any.1, bf16[640,256]{1,0:T(8,128)(2,1)} %v_any.1, bf16[640,256]{1,0:T(8,128)(2,1)} %g_any.1, f32[2,640]{1,0:T(2,128)} %ld_ref.1, f32[1,64]{1,0:T(1,128)} %constant.2.clone.freq_ref, bf16[640,2048]{1,0:T(8,128)(2,1)} %res_any.1, ...), custom_call_target="tpu_custom_call" | custom-call | tf_op jit(solution)/shard_map/pallas_call | solution.py:626
  102.2 2.0 %copy.17 = bf16[640,512]{1,0:T(8,128)(2,1)} copy(bf16[640,512]{1,0:T(8,128)(2,1)} %shard_map.145) | data formatting | bytes 1310720

commit v7 on v6

--- a/solution.py
+++ b/solution.py
@@ -218,7 +218,7 @@
         made = pltpu.make_async_copy(src, dst, local_sem.at[len(local)])
         made.start()
         local.append(made)
-    for made in local[:4]:
+    for made in local[:3]:
         made.wait()
     pl.semaphore_wait(barrier, len(peers))
     net = Net(send_sem, recv_sem, at)
@@ -335,6 +335,7 @@
     start(1)
     if DOWN_AT == 0:
         start(2)
+    local[3].wait()
     gather_out(outs_in)
     for made in local[4:]:
         made.wait()

time: 104 us -> 104 us (level)
  no operation moved by 1% of the time
where the time goes in v7:
time: 104 us
  Pallas kernels  102 us (98%)
  local copies, waits for them, and re-layouts  1.97 us (2%)
    pallas_call x1, Pallas kernels, shards(): pl.pallas_call(kernel, out_shape=jax.ShapeDtypeStruct((ROWS, 512), BF16),...  102 us

profile of v7, /device:TPU:1, one launch (start us, length us, event | category | flops | bytes accessed | tf_op | source)
XLA Modules:
  0.0 104.2 jit_solution(8996216962750066826)
XLA Ops:
  0.0 102.2 %shard_map.145 = bf16[640,512]{1,0:T(8,128)(2,1)} custom-call(bf16[640,256]{1,0:T(8,128)(2,1)} %q_any.1, bf16[640,256]{1,0:T(8,128)(2,1)} %k_any.1, bf16[640,256]{1,0:T(8,128)(2,1)} %v_any.1, bf16[640,256]{1,0:T(8,128)(2,1)} %g_any.1, f32[2,640]{1,0:T(2,128)} %ld_ref.1, f32[1,64]{1,0:T(1,128)} %constant.2.clone.freq_ref, bf16[640,2048]{1,0:T(8,128)(2,1)} %res_any.1, ...), custom_call_target="tpu_custom_call" | custom-call | tf_op jit(solution)/shard_map/pallas_call | solution.py:627
  102.2 2.0 %copy.17 = bf16[640,512]{1,0:T(8,128)(2,1)} copy(bf16[640,512]{1,0:T(8,128)(2,1)} %shard_map.145) | data formatting | bytes 1310720
